TPU v7x, 256 devices: a whole 4x4x8 slice. The times are simulated.
256 devices in a mesh: ep: 64 (over z, x, core), tp: 4 (over y).
Axes of the slice: x: 4, y: 4, z: 8, core: 2. Of those that a mesh axis runs over, the one named last changes fastest.
Arguments:
- tokens: bfloat16 [1024, 2048], P('ep'), may hold values from -6 to 6
- norm1_gain: float32 [2048], replicated, may hold values from 0.1 to 1.9
- query_weight: bfloat16 [2048, 512], P(None, 'tp'), may hold values from -0.125 to 0.125
- key_weight: bfloat16 [2048, 256], P(None, 'tp'), may hold values from -0.125 to 0.125
- value_weight: bfloat16 [2048, 256], P(None, 'tp'), may hold values from -0.125 to 0.125
- forget_weight: bfloat16 [2048, 8], P(None, 'tp'), may hold values from -0.125 to 0.125
- forget_bias: float32 [8], P('tp'), may hold values from 0.5 to 4
- out_weight: bfloat16 [512, 2048], P('tp'), may hold values from -0.25 to 0.25
- kv_cache: bfloat16 [1024, 1024, 4, 128], P('ep', None, 'tp'), may hold values from -6 to 6
- log_gates: float32 [1024, 8, 1024], P('ep', 'tp'), may hold values from -1024 to 0, as said below
- lengths: int32 [1024], P('ep'), may hold values from 64 to 1024
- norm2_gain: float32 [2048], replicated, may hold values from 0.1 to 1.9
- routing: int32 [1024, 4], P('ep'), may hold values from 0 to 63, all different within a row; in each aligned block of 16 rows (0 to 15, 16 to 31, ...) at most 3 rows name the same one
- route_weight: float32 [1024, 4], P('ep'), may hold values from 0.1 to 0.6
- expert_gate: bfloat16 [64, 2048, 2048], P('ep', None, 'tp'), may hold values from -0.25 to 0.25
- expert_up: bfloat16 [64, 2048, 2048], P('ep', None, 'tp'), may hold values from -0.25 to 0.25
- expert_down: bfloat16 [64, 2048, 2048], P('ep', 'tp'), may hold values from -0.0625 to 0.0625
- dense_gate: bfloat16 [2048, 4096], P(None, 'ep'), may hold values from -0.25 to 0.25
- dense_up: bfloat16 [2048, 4096], P(None, 'ep'), may hold values from -0.25 to 0.25
- dense_down: bfloat16 [4096, 2048], P('ep'), may hold values from -0.09375 to 0.09375
- dense_mix: float32 [2048], replicated, may hold values from -0.125 to 0.125
Outputs:
- layer_out: bfloat16 [1024, 2048], P(('ep', 'tp'))
Inputs may be any that keep to these rules, and one draw needn't show every extreme that they name: `log_gates`: Non-increasing along the positions. `routing`: each row names 4 different experts. Among the rows of one index of ep (aligned blocks of 16 rows) no expert is named by more than 3 rows, and in every draw some expert is named by exactly 3 rows of some block.
All inputs are finite; a program needn't handle non-finite values.
Results may differ from a plain program's by a relative error of at most 0.011.
Values may be sent and summed in bfloat16 or wider, within the bound.
A program may use at most 128 MiB of HBM per device.

v0:
```python
import jax
import jax.numpy as jnp
from jax import lax
from jax.sharding import PartitionSpec as P

EPS = 1e-05
LIMIT = 7.0
ALPHA = 1.702


def copy_for_each(shard, axis):
    peers = lax.axis_size(axis)
    return lax.all_to_all(
        jnp.broadcast_to(shard[None], (peers, *shard.shape)), axis, 0, 0, tiled=True
    )


def taken_together(shard, axis):
    everything = copy_for_each(shard, axis)
    return jnp.sum(everything, axis=0)


def joined_along(parts, dim):
    shape = list(parts.shape[1:])
    shape[dim] *= parts.shape[0]
    return jnp.moveaxis(parts, 0, dim).reshape(shape)


def collect(shard, axis, dim):
    return joined_along(copy_for_each(shard, axis), dim)


def items_in_groups(shard, axis, split_dim, concat_dim, work, item_dim, out_dim):

    def moved(group):
        return lax.all_to_all(group, axis, split_axis=split_dim, concat_axis=concat_dim, tiled=True)

    items = jax.tree.leaves(shard)[0].shape[item_dim]
    ends = [items * k // 2 for k in range(2 + 1)] if items % 2 == 0 else [0, items]
    groups = [
        jax.tree.map(lambda a: lax.slice_in_dim(a, low, high, axis=item_dim), shard)
        for low, high in zip(ends, ends[1:])
    ]
    arrived = [moved(group) for group in groups]
    made = [work(group) for group in arrived]
    return jax.tree.map(lambda *parts: jnp.concatenate(parts, axis=out_dim), *made)


def cut_along(shard, dim, peers):
    before, after = (shard.shape[:dim], shard.shape[dim + 1 :])
    return jnp.moveaxis(shard.reshape(*before, peers, -1, *after), dim, 0)


def sent_and_summed(shard, axis, dim):
    parts = cut_along(shard, dim, lax.axis_size(axis))
    arrived = lax.all_to_all(parts, axis, split_axis=0, concat_axis=0, tiled=True)
    return arrived.astype(jnp.float32).sum(axis=0)


def clamped_unit(gate_pre, up_pre):
    capped = jnp.minimum(gate_pre, LIMIT)
    return capped * jax.nn.sigmoid(ALPHA * capped) * (jnp.clip(up_pre, -LIMIT, LIMIT) + 1.0)


def rms_scaled(values, gain_vec):
    return values * lax.rsqrt(jnp.mean(values * values, axis=-1, keepdims=True) + EPS) * gain_vec


def slot_tables(routes, experts, capacity):
    flat_ids = routes.reshape(-1)
    onehot = (flat_ids[:, None] == jnp.arange(experts, dtype=jnp.int32)[None, :]).astype(jnp.int32)
    earlier = jnp.cumsum(onehot, axis=0, dtype=jnp.int32) - onehot
    slot_ids = jnp.sum(earlier * onehot, axis=1, dtype=jnp.int32)
    matches = onehot[:, :, None] * (
        slot_ids[:, None, None] == jnp.arange(capacity, dtype=jnp.int32)[None, None, :]
    ).astype(jnp.int32)
    owners = jnp.arange(flat_ids.shape[0], dtype=jnp.int32) // routes.shape[1]
    source = jnp.sum(matches * owners[:, None, None], axis=0, dtype=jnp.int32)
    return (slot_ids, source)


def on_device(
    tokens,
    norm1_gain,
    query_weight,
    key_weight,
    value_weight,
    forget_weight,
    forget_bias,
    out_weight,
    kv_cache,
    log_gates,
    lengths,
    norm2_gain,
    routing,
    route_weight,
    expert_gate,
    expert_up,
    expert_down,
    dense_gate,
    dense_up,
    dense_down,
    dense_mix,
):
    seq_count, model_width = tokens.shape
    tp_count = lax.axis_size("tp")
    ep_count = lax.axis_size("ep")
    own_rows = seq_count // tp_count
    row_start = lax.axis_index("tp") * own_rows
    local_heads = forget_bias.shape[0]
    kv_local = kv_cache.shape[2]
    head_dim = kv_cache.shape[3] // 2
    per_kv = local_heads // kv_local
    cache_len = kv_cache.shape[1]
    score_scale = head_dim ** (-0.5)
    normed = rms_scaled(tokens.astype(jnp.float32), norm1_gain).astype(jnp.bfloat16)
    queries = jnp.dot(normed, query_weight, preferred_element_type=jnp.float32).astype(jnp.bfloat16)
    queries = queries.reshape(seq_count, kv_local, per_kv, head_dim)
    key_new = jnp.dot(normed, key_weight, preferred_element_type=jnp.float32).astype(jnp.bfloat16)
    key_new = key_new.reshape(seq_count, kv_local, head_dim)
    value_new = jnp.dot(normed, value_weight, preferred_element_type=jnp.float32).astype(
        jnp.bfloat16
    )
    value_new = value_new.reshape(seq_count, kv_local, head_dim)
    gate_new = jax.nn.log_sigmoid(
        jnp.dot(normed, forget_weight, preferred_element_type=jnp.float32) + forget_bias
    )
    scores = (
        jnp.einsum(
            "skgd,slkd->skgl", queries, kv_cache[..., :head_dim], preferred_element_type=jnp.float32
        )
        * score_scale
    )
    last_index = jnp.broadcast_to((lengths - 1)[:, None, None], (seq_count, local_heads, 1))
    last_gate = jnp.take_along_axis(log_gates, last_index, axis=2)
    gate_bias = (last_gate - log_gates + gate_new[:, :, None]).reshape(
        seq_count, kv_local, per_kv, cache_len
    )
    live_mask = (jnp.arange(cache_len, dtype=jnp.int32)[None, :] < lengths[:, None])[
        :, None, None, :
    ]
    cached = jnp.where(live_mask, jnp.exp(scores + gate_bias), 0.0)
    own_exp = jnp.exp(
        jnp.einsum("skgd,skd->skg", queries, key_new, preferred_element_type=jnp.float32)
        * score_scale
    )
    denominator = jnp.sum(cached, axis=-1) + own_exp
    weight_cache = (cached / denominator[..., None]).astype(jnp.bfloat16)
    weight_own = (own_exp / denominator).astype(jnp.bfloat16)
    attended = jnp.einsum(
        "skgl,slkd->skgd",
        weight_cache,
        kv_cache[..., head_dim:],
        preferred_element_type=jnp.float32,
    )
    attended = (
        attended
        + weight_own.astype(jnp.float32)[..., None] * value_new.astype(jnp.float32)[:, :, None, :]
    )
    attended = attended.astype(jnp.bfloat16).reshape(seq_count, local_heads * head_dim)
    partial_out = jnp.dot(attended, out_weight, preferred_element_type=jnp.float32)
    attn_out = taken_together(partial_out, "tp").astype(jnp.bfloat16)
    residual = tokens.astype(jnp.float32) + attn_out.astype(jnp.float32)
    hidden_in = rms_scaled(residual, norm2_gain).astype(jnp.bfloat16)
    own_hidden = lax.dynamic_slice_in_dim(hidden_in, row_start, own_rows, 0)
    own_residual = lax.dynamic_slice_in_dim(residual, row_start, own_rows, 0)
    row_piece = collect(own_hidden, "ep", 0)
    gate_pre = jnp.dot(row_piece, dense_gate, preferred_element_type=jnp.float32)
    up_pre = jnp.dot(row_piece, dense_up, preferred_element_type=jnp.float32)
    dense_act = clamped_unit(gate_pre, up_pre).astype(jnp.bfloat16)
    own_act = lax.all_to_all(dense_act, "ep", split_axis=0, concat_axis=1, tiled=True)
    dense_val = jnp.dot(
        own_act,
        lax.all_gather(dense_down, "ep", axis=0, tiled=True),
        preferred_element_type=jnp.float32,
    )
    local_experts = expert_gate.shape[0]
    experts = local_experts * ep_count
    top_count = routing.shape[1]
    capacity = min(seq_count, seq_count * top_count * 3 // experts)
    slot_ids, source = slot_tables(routing, experts, capacity)
    dispatch = hidden_in[source.reshape(-1)].reshape(experts, capacity, model_width)

    def expert_units(received):
        item_count = received.shape[1]
        grouped = received.reshape(ep_count, local_experts, item_count, model_width)
        gate_pre = jnp.einsum(
            "sjnd,jdf->sjnf", grouped, expert_gate, preferred_element_type=jnp.float32
        )
        up_pre = jnp.einsum(
            "sjnd,jdf->sjnf", grouped, expert_up, preferred_element_type=jnp.float32
        )
        activation = clamped_unit(gate_pre, up_pre).astype(jnp.bfloat16)
        partial_units = jnp.einsum(
            "sjnf,jfd->sjnd", activation, expert_down, preferred_element_type=jnp.float32
        )
        return partial_units.reshape(ep_count * local_experts, item_count, model_width)

    partial_units = items_in_groups(dispatch, "ep", 0, 0, expert_units, 1, 1)
    slot_index = routing * capacity + slot_ids.reshape(seq_count, top_count)
    shares = sent_and_summed(partial_units.astype(jnp.bfloat16), "tp", 2).astype(jnp.bfloat16)
    returned = lax.all_to_all(shares, "ep", split_axis=0, concat_axis=0, tiled=True)
    share_width = returned.shape[2]
    picked = returned.reshape(experts * capacity, share_width)[slot_index.reshape(-1)]
    picked = picked.reshape(seq_count, top_count, share_width)
    moe_cols = jnp.sum(route_weight[..., None] * picked.astype(jnp.float32), axis=1)
    moe_val = lax.all_to_all(
        moe_cols.astype(jnp.bfloat16), "tp", split_axis=0, concat_axis=1, tiled=True
    ).astype(moe_cols.dtype)
    mix_gate = jax.nn.sigmoid(
        jnp.dot(own_hidden.astype(jnp.float32), dense_mix, precision=lax.Precision.HIGHEST)
    )
    return (own_residual + moe_val + mix_gate[:, None] * dense_val).astype(jnp.bfloat16)


def solution(mesh):
    return jax.shard_map(
        on_device,
        mesh=mesh,
        in_specs=(
            P("ep", None),
            P(),
            P(None, "tp"),
            P(None, "tp"),
            P(None, "tp"),
            P(None, "tp"),
            P("tp"),
            P("tp", None),
            P("ep", None, "tp", None),
            P("ep", "tp", None),
            P("ep"),
            P(),
            P("ep", None),
            P("ep", None),
            P("ep", None, "tp"),
            P("ep", None, "tp"),
            P("ep", "tp", None),
            P(None, "ep"),
            P(None, "ep"),
            P("ep", None),
            P(),
        ),
        out_specs=P(("ep", "tp"), None),
        check_vma=False,
    )
```

profile of v0, /device:TPU:1, one launch (start us, length us, event | category | flops | bytes accessed | tf_op | source)
XLA Modules:
  0.0 200.8 jit_solution(5175748005249911537)
XLA Ops:
  6.5 0.7 all-gather.2.cloned.1.call-update
  7.3 0.7 broadcast_compare_fusion
  7.9 0.7 broadcast_add_fusion
  8.9 0.8 gather_fusion.2
  10.0 0.2 convolution_convert_fusion.3
  10.3 0.2 fusion.94
  10.6 0.2 fusion.57
  11.2 3.6 %fusion.109 = (f32[16,2]{1,0:T(8,128)S(1)}, f32[16,2,1024]{2,1,0:T(2,128)S(1)}) fusion(f32[16,2]{1,0:T(8,128)S(1)} %copy.69, f32[16,2,1024]{2,1,0:T(2,128)S(1)} %copy-done.1, f32[16,2]{1,0:T(8,128)S(1)} %fusion.88, bf16[16,2,64]{2,1,0:T(2,128)(2,1)S(1)} %reshape.436, bf16[16,1024,1,128]{3,1,2,0:T(8,128)(2,1)} %param.29, ...), kind=kOutput, calls=%fused_computation.124 | convolution fusion | flops 4390880 | bytes 4477312 | tf_op jit(solution)/shard_map/skgd,slkd->skgl/dot_general | solution.py:129
  14.8 0.2 fusion.56
  15.1 1.4 fusion.53
  16.5 0.2 fusion.110
  16.7 0.8 broadcast_in_dim.41
  17.6 5.0 %all-to-all-start = ((f32[4,16,2048]{2,1,0:T(8,128)}), f32[4,16,2048]{2,1,0:T(8,128)S(1)}, u32[]{:S(2)}, u32[]{:S(2)}) async-start(f32[4,16,2048]{2,1,0:T(8,128)} %broadcast_in_dim.41), calls=%async_computation | async-start | bytes 1048576 | tf_op jit(solution)/shard_map/all_to_all | solution.py:13
  22.9 0.2 select_reduce_fusion
  23.5 6.7 %all-to-all-done = f32[4,16,2048]{2,1,0:T(8,128)S(1)} async-done(((f32[4,16,2048]{2,1,0:T(8,128)}), f32[4,16,2048]{2,1,0:T(8,128)S(1)}, u32[]{:S(2)}, u32[]{:S(2)}) %all-to-all-start) | async-done | bytes 524320 | tf_op jit(solution)/shard_map/all_to_all | solution.py:13
  30.5 1.1 gather_fusion
  31.6 1.3 reshape.441
  32.9 14.3 %all-to-all-start.1 = ((bf16[64,3,2048]{2,1,0:T(4,128)(2,1)}), bf16[64,3,2048]{2,1,0:T(4,128)(2,1)S(1)}, u32[]{:S(2)}, u32[]{:S(2)}) async-start(bf16[64,3,2048]{2,1,0:T(4,128)(2,1)} %reshape.441), calls=%async_computation.1 | async-start | bytes 2097152 | tf_op jit(solution)/shard_map/all_to_all | solution.py:36
  47.2 29.1 %all-to-all-done.1 = bf16[64,3,2048]{2,1,0:T(4,128)(2,1)S(1)} async-done(((bf16[64,3,2048]{2,1,0:T(4,128)(2,1)}), bf16[64,3,2048]{2,1,0:T(4,128)(2,1)S(1)}, u32[]{:S(2)}, u32[]{:S(2)}) %all-to-all-start.1) | async-done | bytes 786464 | tf_op jit(solution)/shard_map/all_to_all | solution.py:36
  76.4 1.5 broadcast_in_dim.42
  77.8 8.1 %all-to-all-start.5 = ((bf16[64,4,2048]{2,1,0:T(4,128)(2,1)}), bf16[64,4,2048]{2,1,0:T(4,128)(2,1)S(1)}, u32[]{:S(2)}, u32[]{:S(2)}) async-start(bf16[64,4,2048]{2,1,0:T(4,128)(2,1)} %broadcast_in_dim.42), calls=%async_computation.5 | async-start | bytes 2097152 | tf_op jit(solution)/shard_map/all_to_all | solution.py:13
  85.9 3.5 %fusion.29 = f32[64,1,3,512]{3,0,2,1:T(8,128)} fusion(bf16[1,2048,512]{2,1,0:T(8,128)(2,1)} %param.35, bf16[64,3,2048]{2,1,0:T(4,128)(2,1)} %copy-done.3), kind=kOutput, calls=%fused_computation.24 | convolution fusion | flops 402751488 | bytes 3276800 | tf_op jit(solution)/shard_map/sjnd,jdf->sjnf/dot_general | solution.py:187
  89.5 4.5 %fusion.6 = bf16[64,1,3,2048]{3,0,2,1:T(8,128)(2,1)} fusion(bf16[1,512,2048]{2,1,0:T(8,128)(2,1)S(1)} %copy-done, bf16[1,2048,512]{2,1,0:T(8,128)(2,1)} %param.36, bf16[64,3,2048]{2,1,0:T(4,128)(2,1)} %copy-done.3, f32[64,1,3,512]{3,0,2,1:T(8,128)} %fusion.29), kind=kOutput, calls=%fused_computation.10 | convolution fusion | flops 806584320 | bytes 6160384 | tf_op jit(solution)/shard_map/sjnf,jfd->sjnd/dot_general | solution.py:194
  94.0 3.0 %convert_element_type.130 = bf16[64,3,4,512]{3,2,0,1:T(4,128)(2,1)} reshape(bf16[64,1,3,2048]{3,0,2,1:T(8,128)(2,1)} %fusion.6) | data formatting | bytes 1572864 | tf_op jit(solution)/shard_map/convert_element_type | solution.py:201
  97.0 2.2 %copy.95 = bf16[64,3,4,512]{3,0,1,2:T(8,128)(2,1)} copy(bf16[64,3,4,512]{3,2,0,1:T(4,128)(2,1)} %convert_element_type.130) | data formatting | bytes 1572864 | tf_op jit(solution)/shard_map/convert_element_type | solution.py:201
  99.2 26.5 %all-to-all-done.5 = bf16[64,4,2048]{2,1,0:T(4,128)(2,1)S(1)} async-done(((bf16[64,4,2048]{2,1,0:T(4,128)(2,1)}), bf16[64,4,2048]{2,1,0:T(4,128)(2,1)S(1)}, u32[]{:S(2)}, u32[]{:S(2)}) %all-to-all-start.5) | async-done | bytes 1048608 | tf_op jit(solution)/shard_map/all_to_all | solution.py:13
  125.8 4.2 %all-to-all-start.2 = ((bf16[4,64,3,512]{3,1,2,0:T(8,128)(2,1)}), bf16[4,64,3,512]{3,1,2,0:T(8,128)(2,1)}, u32[]{:S(2)}, u32[]{:S(2)}) async-start(bf16[4,64,3,512]{3,1,2,0:T(8,128)(2,1)} %bitcast.132), calls=%async_computation.2 | async-start | bytes 1572864 | tf_op jit(solution)/shard_map/all_to_all | solution.py:56
  130.2 0.7 copy.71
  130.8 0.6 pad_clamp_fusion
  131.4 1.1 reshape.449
  132.5 8.8 %all-to-all-done.2 = bf16[4,64,3,512]{3,1,2,0:T(8,128)(2,1)} async-done(((bf16[4,64,3,512]{3,1,2,0:T(8,128)(2,1)}), bf16[4,64,3,512]{3,1,2,0:T(8,128)(2,1)}, u32[]{:S(2)}, u32[]{:S(2)}) %all-to-all-start.2) | async-done | bytes 786464 | tf_op jit(solution)/shard_map/all_to_all | solution.py:56
  141.3 1.3 reduce_sum.81
  142.6 0.9 copy.78
  143.5 7.1 %all-to-all-start.3 = ((bf16[64,3,512]{2,1,0:T(4,128)(2,1)}), bf16[64,3,512]{2,1,0:T(4,128)(2,1)S(1)}, u32[]{:S(2)}, u32[]{:S(2)}) async-start(bf16[64,3,512]{2,1,0:T(4,128)(2,1)} %copy.78), calls=%async_computation.3 | async-start | bytes 524288 | tf_op jit(solution)/shard_map/all_to_all | solution.py:202
  150.6 1.4 convolution_minimum_fusion
  152.0 2.0 fusion.49
  154.0 0.9 copy.80
  154.9 0.7 reshape.485
  155.6 8.1 %all-to-all-done.3 = bf16[64,3,512]{2,1,0:T(4,128)(2,1)S(1)} async-done(((bf16[64,3,512]{2,1,0:T(4,128)(2,1)}), bf16[64,3,512]{2,1,0:T(4,128)(2,1)S(1)}, u32[]{:S(2)}, u32[]{:S(2)}) %all-to-all-start.3) | async-done | bytes 196640 | tf_op jit(solution)/shard_map/all_to_all | solution.py:202
  163.7 4.8 %all-to-all-start.6 = ((bf16[64,2,128]{2,1,0:T(2,128)(2,1)}), bf16[64,2,128]{2,1,0:T(2,128)(2,1)S(1)}, u32[]{:S(2)}, u32[]{:S(2)}) async-start(bf16[64,2,128]{2,1,0:T(2,128)(2,1)} %reshape.485), calls=%async_computation.6 | async-start | bytes 65536 | tf_op jit(solution)/shard_map/all_to_all | solution.py:171
  168.6 0.8 gather_fusion.1
  169.5 0.9 multiply_reduce_fusion
  170.4 0.6 convert_element_type.134
  171.0 6.9 %all-to-all-done.6 = bf16[64,2,128]{2,1,0:T(2,128)(2,1)S(1)} async-done(((bf16[64,2,128]{2,1,0:T(2,128)(2,1)}), bf16[64,2,128]{2,1,0:T(2,128)(2,1)S(1)}, u32[]{:S(2)}, u32[]{:S(2)}) %all-to-all-start.6) | async-done | bytes 32800 | tf_op jit(solution)/shard_map/all_to_all | solution.py:171
  177.9 3.3 %all-to-all-start.4 = ((bf16[4,4,512]{2,1,0:T(4,128)(2,1)}), bf16[4,4,512]{2,1,0:T(4,128)(2,1)S(1)}, u32[]{:S(2)}, u32[]{:S(2)}) async-start(bf16[4,4,512]{2,1,0:T(4,128)(2,1)} %convert_element_type.134), calls=%async_computation.4 | async-start | bytes 32768 | tf_op jit(solution)/shard_map/all_to_all | solution.py:207
  181.1 0.8 fusion.62
  182.3 3.1 %all-to-all-done.4 = bf16[4,4,512]{2,1,0:T(4,128)(2,1)S(1)} async-done(((bf16[4,4,512]{2,1,0:T(4,128)(2,1)}), bf16[4,4,512]{2,1,0:T(4,128)(2,1)S(1)}, u32[]{:S(2)}, u32[]{:S(2)}) %all-to-all-start.4) | async-done | bytes 16416 | tf_op jit(solution)/shard_map/all_to_all | solution.py:207
  185.3 8.7 %fusion.8 = bf16[4,2048]{1,0:T(4,128)(2,1)} fusion(bf16[4,4096]{1,0:T(4,128)(2,1)S(1)} %all_to_all.46, bf16[4096,2048]{1,0:T(8,128)(2,1)} %all-gather.2.cloned.1.call-done, f32[4,2048]{1,0:T(4,128)S(1)} %bitcast.135, f32[16,2048]{1,0:T(8,128)S(1)} %get-tuple-element.6, s32[]{:T(128)S(6)} %select_n.83, f32[4]{0:T(128)S(1)} %fusion.62), kind=kOutput, calls=%fused_computation.13 | convolution fusion | flops 67141632 | bytes 16891924 | tf_op jit(solution)/shard_map/dot_general | solution.py:172
  (79 shorter events, 2.8 us)
Async XLA Ops:
  6.5 82.9 %copy-start = (bf16[1,512,2048]{2,1,0:T(8,128)(2,1)S(1)}, bf16[1,512,2048]{2,1,0:T(8,128)(2,1)}, u32[]{:S(2)}) copy-start(bf16[1,512,2048]{2,1,0:T(8,128)(2,1)} %param.37) | copy-start | bytes 6291460
  6.5 2.3 %copy-start.1 = (f32[16,2,1024]{2,1,0:T(2,128)S(1)}, f32[16,2,1024]{2,1,0:T(2,128)}, u32[]{:S(2)}) copy-start(f32[16,2,1024]{2,1,0:T(2,128)} %param.30) | copy-start | bytes 393220
  6.5 178.8 %all-gather.2.cloned.1.call-start = ((), (), s32[]{:S(2)}) async-start(), calls=%async_computation.7 | async-start | bytes 17039360 | tf_op jit(solution)/shard_map/all_gather | solution.py:174
  8.8 1.0 copy-start.4
  8.8 1.1 copy-start.6
  8.8 1.1 copy-start.7
  8.8 1.4 copy-start.15
  8.9 1.4 copy-start.16
  8.9 1.7 copy-start.13
  8.9 2.0 copy-start.11
  11.1 3.7 %copy-start.14 = (bf16[2048,64]{0,1:T(8,128)(2,1)S(1)}, bf16[2048,64]{0,1:T(8,128)(2,1)}, u32[]{:S(2)}) copy-start(bf16[2048,64]{0,1:T(8,128)(2,1)} %param.25) | copy-start | bytes 786436
  11.2 3.9 %copy-start.12 = (bf16[16,1024,1,128]{3,1,2,0:T(8,128)(2,1)S(1)}, bf16[16,1024,1,128]{3,1,2,0:T(8,128)(2,1)}, u32[]{:S(2)}) copy-start(bf16[16,1024,1,128]{3,1,2,0:T(8,128)(2,1)} %param.29) | copy-start | bytes 12582916
  15.0 1.5 copy-start.5
  16.4 6.1 %copy-start.9 = (s32[16,4]{0,1:T(4,128)S(1)}, s32[16,4]{0,1:T(4,128)}, u32[]{:S(2)}) copy-start(s32[16,4]{0,1:T(4,128)} %param.33) | copy-start | bytes 772
  16.4 13.9 %copy-start.8 = (f32[2048]{0:T(1024)S(1)}, f32[2048]{0:T(1024)}, u32[]{:S(2)}) copy-start(f32[2048]{0:T(1024)} %param.32) | copy-start | bytes 24580
  17.6 12.6 %all-to-all-start = ((f32[4,16,2048]{2,1,0:T(8,128)}), f32[4,16,2048]{2,1,0:T(8,128)S(1)}, u32[]{:S(2)}, u32[]{:S(2)}) async-start(f32[4,16,2048]{2,1,0:T(8,128)} %broadcast_in_dim.41), calls=%async_computation | async-start | bytes 1048576 | tf_op jit(solution)/shard_map/all_to_all | solution.py:13
  32.9 43.4 %all-to-all-start.1 = ((bf16[64,3,2048]{2,1,0:T(4,128)(2,1)}), bf16[64,3,2048]{2,1,0:T(4,128)(2,1)S(1)}, u32[]{:S(2)}, u32[]{:S(2)}) async-start(bf16[64,3,2048]{2,1,0:T(4,128)(2,1)} %reshape.441), calls=%async_computation.1 | async-start | bytes 2097152 | tf_op jit(solution)/shard_map/all_to_all | solution.py:36
  76.4 1.5 copy-start.3
  77.8 47.9 %all-to-all-start.5 = ((bf16[64,4,2048]{2,1,0:T(4,128)(2,1)}), bf16[64,4,2048]{2,1,0:T(4,128)(2,1)S(1)}, u32[]{:S(2)}, u32[]{:S(2)}) async-start(bf16[64,4,2048]{2,1,0:T(4,128)(2,1)} %broadcast_in_dim.42), calls=%async_computation.5 | async-start | bytes 2097152 | tf_op jit(solution)/shard_map/all_to_all | solution.py:13
  94.0 36.2 %copy-start.10 = (f32[16,4]{0,1:T(4,128)S(1)}, f32[16,4]{0,1:T(4,128)}, u32[]{:S(2)}) copy-start(f32[16,4]{0,1:T(4,128)} %param.34) | copy-start | bytes 772
  125.8 15.6 %all-to-all-start.2 = ((bf16[4,64,3,512]{3,1,2,0:T(8,128)(2,1)}), bf16[4,64,3,512]{3,1,2,0:T(8,128)(2,1)}, u32[]{:S(2)}, u32[]{:S(2)}) async-start(bf16[4,64,3,512]{3,1,2,0:T(8,128)(2,1)} %bitcast.132), calls=%async_computation.2 | async-start | bytes 1572864 | tf_op jit(solution)/shard_map/all_to_all | solution.py:56
  132.5 18.1 %copy-start.2 = (bf16[256,2048]{1,0:T(8,128)(2,1)S(1)}, bf16[256,2048]{1,0:T(8,128)(2,1)}, u32[]{:S(2)}) copy-start(bf16[256,2048]{1,0:T(8,128)(2,1)} %reshape.449) | copy-start | bytes 3145732
  143.5 20.2 %all-to-all-start.3 = ((bf16[64,3,512]{2,1,0:T(4,128)(2,1)}), bf16[64,3,512]{2,1,0:T(4,128)(2,1)S(1)}, u32[]{:S(2)}, u32[]{:S(2)}) async-start(bf16[64,3,512]{2,1,0:T(4,128)(2,1)} %copy.78), calls=%async_computation.3 | async-start | bytes 524288 | tf_op jit(solution)/shard_map/all_to_all | solution.py:202
  163.7 14.2 %all-to-all-start.6 = ((bf16[64,2,128]{2,1,0:T(2,128)(2,1)}), bf16[64,2,128]{2,1,0:T(2,128)(2,1)S(1)}, u32[]{:S(2)}, u32[]{:S(2)}) async-start(bf16[64,2,128]{2,1,0:T(2,128)(2,1)} %reshape.485), calls=%async_computation.6 | async-start | bytes 65536 | tf_op jit(solution)/shard_map/all_to_all | solution.py:171
  177.9 7.4 %all-to-all-start.4 = ((bf16[4,4,512]{2,1,0:T(4,128)(2,1)}), bf16[4,4,512]{2,1,0:T(4,128)(2,1)S(1)}, u32[]{:S(2)}, u32[]{:S(2)}) async-start(bf16[4,4,512]{2,1,0:T(4,128)(2,1)} %convert_element_type.134), calls=%async_computation.4 | async-start | bytes 32768 | tf_op jit(solution)/shard_map/all_to_all | solution.py:207
Sparse Core Ops, SparseCore 0:
  10.1 131.2 all-gather.1
where the time goes:
time: 202 us; the launch traced here: 201 us
  waiting for transfers between devices  89.9 us (45%)
  starting transfers between devices  46.7 us (23%)
  matrix products  27.1 us (13%)
  local copies, waits for them, and re-layouts  18.2 us (9%)
  between operations  13.8 us (7%)
  other arithmetic  5.16 us (3%)
    all_to_all x2, waiting for transfers between devices, copy_for_each(): lax.all_to_all(jnp.broadcast_to(shard[None], (peers, *shard.shape)), axis...  33.2 us
    all_to_all x1, waiting for transfers between devices, moved(): lax.all_to_all(group, axis, split_axis=split_dim, concat_axis=concat_dim,...  29.1 us
    all_to_all x1, starting transfers between devices, moved(): lax.all_to_all(group, axis, split_axis=split_dim, concat_axis=concat_dim,...  14.3 us
    all_to_all x2, starting transfers between devices, copy_for_each(): lax.all_to_all(jnp.broadcast_to(shard[None], (peers, *shard.shape)), axis...  13.1 us
    all_to_all x1, waiting for transfers between devices, sent_and_summed(): lax.all_to_all(parts, axis, split_axis=0, concat_axis=0, tiled=True)  8.78 us
    dot_general x1, matrix products, on_device(): jnp.dot(own_act, lax.all_gather(dense_down, 'ep', axis=0, tiled=True), pr...  8.65 us
    all_to_all x1, waiting for transfers between devices, on_device(): lax.all_to_all(shares, 'ep', split_axis=0, concat_axis=0, tiled=True)  8.09 us
    all_to_all x1, starting transfers between devices, on_device(): lax.all_to_all(shares, 'ep', split_axis=0, concat_axis=0, tiled=True)  7.11 us
  transfers between devices with their start and end apart: 8, of which 7 were waited for; matrix products, arithmetic and copies ran while one was open for 21% of the time, Pallas kernels for 0%

commit v1 on v0

v1 whole, which is shorter than its diff:
```python
import functools

import jax
import jax.numpy as jnp
import numpy as np
from jax import lax
from jax.experimental import pallas as pl
from jax.experimental.pallas import tpu as pltpu
from jax.sharding import PartitionSpec as P

EPS = 1e-05
LIMIT = 7.0
ALPHA = 1.702
NZ, NX, NC = 8, 4, 2
CAP = 3
META = 128
MESH = pl.DeviceIdType.MESH


def clamped_unit(gate_pre, up_pre):
    capped = jnp.minimum(gate_pre, LIMIT)
    return capped * jax.nn.sigmoid(ALPHA * capped) * (jnp.clip(up_pre, -LIMIT, LIMIT) + 1.0)


def rms_scaled(values, gain_vec):
    return values * lax.rsqrt(jnp.mean(values * values, axis=-1, keepdims=True) + EPS) * gain_vec


def remote(src, dst, send_sem, recv_sem, **device):
    return pltpu.make_async_remote_copy(
        src_ref=src,
        dst_ref=dst,
        send_sem=send_sem,
        recv_sem=recv_sem,
        device_id=device,
        device_id_type=MESH,
    )


def layer_kernel(
    top,
    part,
    tok,
    gain2,
    meta,
    dmix,
    gs,
    cb,
    own_xc,
    eg_hbm,
    eu_hbm,
    ed_hbm,
    wlo_hbm,
    whi_hbm,
    dd_hbm,
    out,
    h_all,
    eg,
    eu,
    ed,
    wlo,
    whi,
    dd,
    s1buf,
    yb,
    resid,
    pick,
    xs,
    ysend,
    yrecv,
    rown,
    zs,
    zr,
    zf,
    asend,
    arecv,
    cs,
    c32,
    cr,
    fs,
    fr,
    ldsem,
    s1s,
    s1r,
    s2s,
    s2r,
    xss,
    xrs,
    rss,
    rrs,
    lss,
    lrs,
    dcs,
    dcr,
    dds,
    ddr,
    yss,
    yrs,
    zss,
    zrs,
    ass,
    ars,
    css,
    crs,
    fss,
    frs,
):
    ny, rows4, d_model = part.shape
    seq = meta.shape[0]
    nblk = NC * NZ * NX
    n_rows = nblk * seq
    fq = d_model // ny
    nxc = NX * NC
    zrows = CAP * nxc
    f32, bf16 = jnp.float32, jnp.bfloat16
    ep = lax.axis_index("ep")
    t = lax.axis_index("tp")
    z = ep // nxc
    x = (ep // NC) % NX
    c = ep % NC

    def ep_at(zi, xi, ci):
        return (zi * NX + xi) * NC + ci

    def blk(ci, zi, xi):
        return (ci * NZ + zi) * NX + xi

    def yp(d):
        return lax.rem(t + d + ny, ny)

    def zp(d):
        return lax.rem(z + d + NZ, NZ)

    def xp(d):
        return lax.rem(x + d + NX, NX)

    def cp(d):
        return lax.rem(c + d, NC)

    xc_rel = [(dx, dc) for dc in range(NC) for dx in range(NX) if dx or dc]

    barrier = pltpu.get_barrier_semaphore()
    for d in range(1, ny):
        pl.semaphore_signal(barrier, inc=1, device_id={"tp": yp(d)}, device_id_type=MESH)
    for dx, dc in xc_rel:
        pl.semaphore_signal(
            barrier, inc=1, device_id={"ep": ep_at(z, xp(dx), cp(dc))}, device_id_type=MESH
        )
    for d in range(1, NZ):
        pl.semaphore_signal(
            barrier, inc=1, device_id={"ep": ep_at(zp(d), x, c)}, device_id_type=MESH
        )

    loads = [
        pltpu.make_async_copy(src, dst, ldsem.at[i])
        for i, (src, dst) in enumerate(
            [
                (eg_hbm, eg),
                (eu_hbm, eu),
                (ed_hbm, ed),
                (wlo_hbm, wlo),
                (whi_hbm, whi),
                (dd_hbm.at[:, pl.ds(pl.multiple_of(t * fq, fq), fq)], dd.at[z, 0]),
            ]
        )
    ]
    for load in loads:
        load.start()
    pl.semaphore_wait(barrier, (ny - 1) + len(xc_rel) + (NZ - 1))

    sent = []

    def go(copy):
        copy.start()
        sent.append(copy)

    firsts = [
        remote(part.at[yp(d)], s1buf.at[d - 1], s1s.at[d - 1], s1r.at[d - 1], tp=yp(d))
        for d in range(1, ny)
    ]
    for copy in firsts:
        go(copy)
    total = part[t]
    for d, copy in enumerate(firsts):
        copy.wait_recv()
        total = total + s1buf[d]
    res = tok[t].astype(f32) + total.astype(bf16).astype(f32)
    resid[...] = res
    yb[t] = rms_scaled(res, gain2[...]).astype(bf16)
    for d in range(1, ny):
        go(remote(yb.at[t], yb.at[t], s2s.at[d - 1], s2r.at[d - 1], tp=yp(d)))
    for d in range(1, ny):
        there = yb.at[yp(-d)]
        remote(there, there, s2s.at[d - 1], s2r.at[d - 1], tp=yp(-d)).wait_recv()
    mine = h_all.at[blk(c, z, x)]
    mine[:, :d_model] = jnp.concatenate([yb[j].astype(f32) for j in range(ny)], axis=0).astype(bf16)
    mine[:, d_model:] = meta[...]

    for d in range(1, NX):
        go(remote(mine, mine, xss.at[d - 1], xrs.at[d - 1], ep=ep_at(z, xp(d), c)))

    half = (NX + 1) // 2
    last = NZ // 2

    def takes(direction, step, q):
        if step < last:
            return True
        return q < half if direction > 0 else q >= half

    def pass_on(direction, step, q):
        if step > last or not takes(direction, step, q):
            return
        block = h_all.at[blk(c, zp(-direction * (step - 1)), xp(-q))]
        ss, rs = (rss, rrs) if direction > 0 else (lss, lrs)
        go(
            remote(
                block, block, ss.at[step - 1, q], rs.at[step - 1, q], ep=ep_at(zp(direction), x, c)
            )
        )

    def across(rel, q):
        block = h_all.at[blk(c, zp(rel), xp(-q))]
        i = rel % NZ
        go(remote(block, block, dcs.at[i, q], dcr.at[i, q], ep=ep_at(z, x, cp(1))))

    for q in range(NX):
        if q:
            block = h_all.at[blk(c, z, xp(-q))]
            remote(block, block, xss.at[q - 1], xrs.at[q - 1], ep=ep_at(z, xp(-q), c)).wait_recv()
        pass_on(1, 1, q)
        pass_on(-1, 1, q)
        across(0, q)
    for step in range(1, last + 1):
        for q in range(NX):
            for direction in (1, -1):
                if not takes(direction, step, q):
                    continue
                rs, ss = (rrs, rss) if direction > 0 else (lrs, lss)
                block = h_all.at[blk(c, zp(-direction * step), xp(-q))]
                remote(
                    block,
                    block,
                    ss.at[step - 1, q],
                    rs.at[step - 1, q],
                    ep=ep_at(zp(-direction), x, c),
                ).wait_recv()
                pass_on(direction, step + 1, q)
                across(-direction * step, q)
    for rel in range(NZ):
        for q in range(NX):
            block = h_all.at[blk(cp(1), zp(rel), xp(-q))]
            remote(block, block, dcs.at[rel, q], dcr.at[rel, q], ep=ep_at(z, x, cp(1))).wait_recv()

    for load in loads:
        load.wait()
    for d in range(1, NZ):
        go(
            remote(
                dd.at[z, 0], dd.at[z, 0], dds.at[d - 1], ddr.at[d - 1], ep=ep_at(zp(d), x, c)
            )
        )

    codes = h_all[:, :, d_model:].reshape(n_rows, META)
    lead = lax.broadcasted_iota(jnp.int32, (8, META), 0)
    lane = lax.broadcasted_iota(jnp.int32, (8, META), 1)
    unit = jnp.where(lead == lane, 1.0, 0.0).astype(bf16)
    code_rows = lax.dot_general(
        unit, codes, (((1,), (1,)), ((), ())), preferred_element_type=f32
    )
    slot = jnp.full((1, n_rows), -1.0, f32)
    base = (ep * 4).astype(f32)
    for k in range(top):
        j = code_rows[k : k + 1] - base
        slot = jnp.where((j >= 0.0) & (j <= CAP - 1.0), gs[0:1] + j * nxc, slot)
    slots = NZ * zrows
    order = lax.broadcasted_iota(jnp.int32, (slots, n_rows), 0).astype(f32)
    pick[...] = jnp.where(order == slot, 1.0, 0.0).astype(bf16)
    step_n = min(512, d_model)
    for n in range(0, d_model, step_n):
        xs[:, n : n + step_n] = jnp.dot(
            pick[...],
            h_all[:, :, n : n + step_n].reshape(n_rows, step_n),
            preferred_element_type=f32,
        ).astype(bf16)
    act = clamped_unit(
        jnp.dot(xs[...], eg[...], preferred_element_type=f32),
        jnp.dot(xs[...], eu[...], preferred_element_type=f32),
    ).astype(bf16)

    z_order = sorted(range(NZ), key=lambda d: -min(d, NZ - d))
    y_order = sorted(range(1, ny), key=lambda d: -min(d, ny - d))

    def block_result(peer):
        return jnp.dot(
            act, ed[:, pl.ds(pl.multiple_of(peer * fq, fq), fq)], preferred_element_type=f32
        )

    for d in y_order:
        made = block_result(yp(d))
        for zi in range(NZ):
            ysend[d - 1, zi] = made[zi * zrows : (zi + 1) * zrows].astype(bf16)
        for dz in z_order:
            zi = zp(dz)
            go(
                remote(
                    ysend.at[d - 1, zi],
                    yrecv.at[d - 1, zi],
                    yss.at[d - 1, dz],
                    yrs.at[d - 1, dz],
                    tp=yp(d),
                )
            )
    made = block_result(t)
    for zi in range(NZ):
        rown[zi] = made[zi * zrows : (zi + 1) * zrows]

    per_z = NX * seq
    two_units = wlo.shape[1] // 2
    for zi in range(NZ):
        low = h_all[blk(0, zi, 0) : blk(0, zi, 0) + NX, :, :d_model].reshape(per_z, d_model)
        high = h_all[blk(1, zi, 0) : blk(1, zi, 0) + NX, :, :d_model].reshape(per_z, d_model)
        pre = jnp.dot(low, wlo[...], preferred_element_type=f32) + jnp.dot(
            high, whi[...], preferred_element_type=f32
        )
        asend[zi] = clamped_unit(pre[:, :two_units], pre[:, two_units:]).astype(bf16)
    for dz in z_order[:-1]:
        go(
            remote(
                asend.at[zp(dz)],
                arecv.at[z],
                ass.at[dz - 1],
                ars.at[dz - 1],
                ep=ep_at(zp(dz), x, c),
            )
        )
    arecv[z] = asend[z]

    own_rows = [h_all[pl.ds(blk(ci, z, 0), NX)].reshape(per_z, d_model + META) for ci in range(NC)]
    own_meta = jnp.concatenate([r[:, d_model:].astype(f32) for r in own_rows], axis=0)
    mix = jnp.concatenate(
        [
            jnp.sum(r[:, :d_model].astype(f32) * dmix[...], axis=-1, keepdims=True)
            for r in own_rows
        ],
        axis=0,
    )
    mix = jax.nn.sigmoid(mix)
    targets = cb[0:1] + (4 * (x * NC + c)).astype(f32)
    spread = jnp.zeros((NC * per_z, slots), f32)
    for k in range(top):
        weight = (
            own_meta[:, top + k : top + k + 1]
            + own_meta[:, 2 * top + k : 2 * top + k + 1]
            + own_meta[:, 3 * top + k : 3 * top + k + 1]
        )
        spread = spread + jnp.where(own_meta[:, k : k + 1] == targets, weight, 0.0)
    spread = spread * own_xc[...]
    spread_high = spread.astype(bf16)
    spread_low = (spread - spread_high.astype(f32)).astype(bf16)

    for dz in z_order:
        zi = zp(dz)
        summed = rown[zi]
        for d in range(1, ny):
            there = yrecv.at[d - 1, zi]
            remote(
                ysend.at[d - 1, zi], there, yss.at[d - 1, dz], yrs.at[d - 1, dz], tp=yp(-d)
            ).wait_recv()
            summed = summed + there[...].astype(f32)
        if dz:
            zs[zi] = summed.astype(bf16)
            go(
                remote(
                    zs.at[zi], zr.at[z], zss.at[dz - 1], zrs.at[dz - 1], ep=ep_at(zi, x, c)
                )
            )
        else:
            zr[z] = summed.astype(bf16)

    for d in range(1, NZ):
        there = dd.at[zp(-d), 0]
        remote(there, there, dds.at[d - 1], ddr.at[d - 1], ep=ep_at(zp(-d), x, c)).wait_recv()
    for d in range(1, NZ):
        there = arecv.at[zp(-d)]
        remote(there, there, ass.at[d - 1], ars.at[d - 1], ep=ep_at(zp(-d), x, c)).wait_recv()
    units = two_units // 2
    first = lax.broadcasted_iota(jnp.int32, (per_z, two_units), 1) < units
    dense = jnp.zeros((NC * per_z, fq), f32)
    for j in range(NZ):
        dd[j, 1] = dd[j, 0]
        got = arecv[j].astype(f32)
        both = jnp.concatenate(
            [jnp.where(first, got, 0.0), jnp.where(first, 0.0, got)], axis=0
        ).astype(bf16)
        dense = dense + jnp.dot(
            both, dd[j].reshape(two_units, fq), preferred_element_type=f32
        )
    for d in range(1, NZ):
        there = zr.at[zp(-d)]
        remote(there, there, zss.at[d - 1], zrs.at[d - 1], ep=ep_at(zp(-d), x, c)).wait_recv()
    for j in range(NZ):
        zf[j * zrows : (j + 1) * zrows] = zr[j].astype(f32)
    results = zf[...].astype(bf16)
    mixed = (
        jnp.dot(spread_high, results, preferred_element_type=f32)
        + jnp.dot(spread_low, results, preferred_element_type=f32)
        + mix * dense
    )
    c32[...] = mixed.reshape(nxc, seq, fq)
    cs[...] = mixed.astype(bf16).reshape(nxc, seq, fq)

    def xc_at(xi, ci):
        return ci * NX + xi

    for i, (dx, dc) in enumerate(xc_rel):
        xi, ci = xp(dx), cp(dc)
        go(remote(cs.at[xc_at(xi, ci)], cr.at[i], css.at[i], crs.at[i], ep=ep_at(z, xi, ci)))
    moe = c32[xc_at(x, c)]
    for i, (dx, dc) in enumerate(xc_rel):
        remote(cs.at[0], cr.at[i], css.at[i], crs.at[i], ep=ep_at(z, xp(-dx), cp(dc))).wait_recv()
        moe = moe + cr[i].astype(f32)

    for j in range(ny):
        fs[j] = moe[j * rows4 : (j + 1) * rows4]
    for d in range(1, ny):
        go(remote(fs.at[yp(d)], fr.at[t], fss.at[d - 1], frs.at[d - 1], tp=yp(d)))
    fr[t] = fs[t]
    for d in range(1, ny):
        there = fr.at[yp(-d)]
        remote(fs.at[0], there, fss.at[d - 1], frs.at[d - 1], tp=yp(-d)).wait_recv()
    for j in range(ny):
        cols = slice(j * fq, (j + 1) * fq)
        out[:, cols] = (resid[:, cols] + fr[j]).astype(bf16)
    for copy in sent:
        copy.wait_send()


def after_attention(
    partial_out,
    tokens,
    norm2_gain,
    routing,
    route_weight,
    expert_gate,
    expert_up,
    expert_down,
    dense_gate,
    dense_up,
    dense_down,
    dense_mix,
):
    seq, d_model = tokens.shape
    top = routing.shape[1]
    ny = lax.axis_size("tp")
    rows4 = seq // ny
    ff = expert_gate.shape[2]
    units = dense_gate.shape[1]
    fq = d_model // ny
    nxc = NX * NC
    nblk = NC * NZ * NX
    n_rows = nblk * seq
    zrows = CAP * nxc
    slots = NZ * zrows
    f32, bf16 = jnp.float32, jnp.bfloat16

    same = routing[:, :, None, None] == routing[None, None, :, :]
    before = (jnp.arange(seq)[None, :] < jnp.arange(seq)[:, None])[:, None, :, None]
    rank = jnp.sum((same & before).astype(jnp.int32), axis=(2, 3))
    high = lax.reduce_precision(route_weight, 8, 7)
    mid = lax.reduce_precision(route_weight - high, 8, 7)
    low = route_weight - high - mid
    meta = jnp.concatenate([(routing * 4 + rank).astype(f32), high, mid, low], axis=1)
    meta = jnp.pad(meta, ((0, 0), (0, META - 4 * top))).astype(bf16)

    b = np.arange(n_rows) // seq
    bx, bz, bc = b % NX, (b // NX) % NZ, b // (NX * NZ)
    gs = np.broadcast_to((bz * zrows + bx * NC + bc).astype(np.float32), (8, n_rows))
    s = np.arange(slots)
    cb = np.broadcast_to((4 * nxc * (s // zrows) + (s % zrows) // nxc).astype(np.float32), (8, slots))
    r = np.arange(NC * NX * seq) // seq
    own_xc = ((r % NX) * NC + r // NX)[:, None] == (s % nxc)[None, :]

    none = jnp.zeros((d_model, units), bf16)
    wlo = jnp.concatenate([dense_gate, none, dense_up, none], axis=1)
    whi = jnp.concatenate([none, dense_gate, none, dense_up], axis=1)

    dma = pltpu.SemaphoreType.DMA
    vm = pltpu.VMEM
    width = d_model + META
    last = NZ // 2
    scratch = [
        vm((nblk, seq, width), bf16),
        vm((d_model, ff), bf16),
        vm((d_model, ff), bf16),
        vm((ff, d_model), bf16),
        vm((d_model, 4 * units), bf16),
        vm((d_model, 4 * units), bf16),
        vm((NZ, 2, units, fq), bf16),
        vm((ny - 1, rows4, d_model), f32),
        vm((ny, rows4, d_model), bf16),
        vm((rows4, d_model), f32),
        vm((slots, n_rows), bf16),
        vm((slots, d_model), bf16),
        vm((ny - 1, NZ, zrows, fq), bf16),
        vm((ny - 1, NZ, zrows, fq), bf16),
        vm((NZ, zrows, fq), f32),
        vm((NZ, zrows, fq), bf16),
        vm((NZ, zrows, fq), bf16),
        vm((slots, fq), f32),
        vm((NZ, NX * seq, 2 * units), bf16),
        vm((NZ, NX * seq, 2 * units), bf16),
        vm((nxc, seq, fq), bf16),
        vm((nxc, seq, fq), f32),
        vm((nxc - 1, seq, fq), bf16),
        vm((ny, rows4, fq), f32),
        vm((ny, rows4, fq), f32),
        dma((6,)),
    ]
    scratch += [dma((ny - 1,))] * 4
    scratch += [dma((max(NX - 1, 1),))] * 2
    scratch += [dma((last, NX))] * 4
    scratch += [dma((NZ, NX))] * 2
    scratch += [dma((NZ - 1,))] * 2
    scratch += [dma((ny - 1, NZ))] * 2
    scratch += [dma((NZ - 1,))] * 4
    scratch += [dma((nxc - 1,))] * 2
    scratch += [dma((ny - 1,))] * 2
    in_vmem = pl.BlockSpec(memory_space=pltpu.VMEM)
    in_hbm = pl.BlockSpec(memory_space=pl.ANY)
    return pl.pallas_call(
        functools.partial(layer_kernel, top),
        out_shape=jax.ShapeDtypeStruct((rows4, d_model), bf16),
        in_specs=[in_vmem] * 8 + [in_hbm] * 6,
        out_specs=in_vmem,
        scratch_shapes=scratch,
        compiler_params=pltpu.CompilerParams(
            collective_id=0, has_side_effects=True, vmem_limit_bytes=60 * 1024 * 1024
        ),
        name="layer",
    )(
        partial_out.reshape(ny, rows4, d_model),
        tokens.reshape(ny, rows4, d_model),
        norm2_gain.reshape(1, d_model),
        meta,
        dense_mix.reshape(1, d_model),
        jnp.asarray(gs),
        jnp.asarray(cb),
        jnp.asarray(own_xc.astype(np.float32)),
        expert_gate[0],
        expert_up[0],
        expert_down[0],
        wlo,
        whi,
        dense_down,
    )


def on_device(
    tokens,
    norm1_gain,
    query_weight,
    key_weight,
    value_weight,
    forget_weight,
    forget_bias,
    out_weight,
    kv_cache,
    log_gates,
    lengths,
    norm2_gain,
    routing,
    route_weight,
    expert_gate,
    expert_up,
    expert_down,
    dense_gate,
    dense_up,
    dense_down,
    dense_mix,
):
    seq_count, model_width = tokens.shape
    local_heads = forget_bias.shape[0]
    kv_local = kv_cache.shape[2]
    head_dim = kv_cache.shape[3] // 2
    per_kv = local_heads // kv_local
    cache_len = kv_cache.shape[1]
    score_scale = head_dim ** (-0.5)
    normed = rms_scaled(tokens.astype(jnp.float32), norm1_gain).astype(jnp.bfloat16)
    queries = jnp.dot(normed, query_weight, preferred_element_type=jnp.float32).astype(jnp.bfloat16)
    queries = queries.reshape(seq_count, kv_local, per_kv, head_dim)
    key_new = jnp.dot(normed, key_weight, preferred_element_type=jnp.float32).astype(jnp.bfloat16)
    key_new = key_new.reshape(seq_count, kv_local, head_dim)
    value_new = jnp.dot(normed, value_weight, preferred_element_type=jnp.float32).astype(
        jnp.bfloat16
    )
    value_new = value_new.reshape(seq_count, kv_local, head_dim)
    gate_new = jax.nn.log_sigmoid(
        jnp.dot(normed, forget_weight, preferred_element_type=jnp.float32) + forget_bias
    )
    scores = (
        jnp.einsum(
            "skgd,slkd->skgl", queries, kv_cache[..., :head_dim], preferred_element_type=jnp.float32
        )
        * score_scale
    )
    last_index = jnp.broadcast_to((lengths - 1)[:, None, None], (seq_count, local_heads, 1))
    last_gate = jnp.take_along_axis(log_gates, last_index, axis=2)
    gate_bias = (last_gate - log_gates + gate_new[:, :, None]).reshape(
        seq_count, kv_local, per_kv, cache_len
    )
    live_mask = (jnp.arange(cache_len, dtype=jnp.int32)[None, :] < lengths[:, None])[
        :, None, None, :
    ]
    cached = jnp.where(live_mask, jnp.exp(scores + gate_bias), 0.0)
    own_exp = jnp.exp(
        jnp.einsum("skgd,skd->skg", queries, key_new, preferred_element_type=jnp.float32)
        * score_scale
    )
    denominator = jnp.sum(cached, axis=-1) + own_exp
    weight_cache = (cached / denominator[..., None]).astype(jnp.bfloat16)
    weight_own = (own_exp / denominator).astype(jnp.bfloat16)
    attended = jnp.einsum(
        "skgl,slkd->skgd",
        weight_cache,
        kv_cache[..., head_dim:],
        preferred_element_type=jnp.float32,
    )
    attended = (
        attended
        + weight_own.astype(jnp.float32)[..., None] * value_new.astype(jnp.float32)[:, :, None, :]
    )
    attended = attended.astype(jnp.bfloat16).reshape(seq_count, local_heads * head_dim)
    partial_out = jnp.dot(attended, out_weight, preferred_element_type=jnp.float32)
    return after_attention(
        partial_out,
        tokens,
        norm2_gain,
        routing,
        route_weight,
        expert_gate,
        expert_up,
        expert_down,
        dense_gate,
        dense_up,
        dense_down,
        dense_mix,
    )


def solution(mesh):
    return jax.shard_map(
        on_device,
        mesh=mesh,
        in_specs=(
            P("ep", None),
            P(),
            P(None, "tp"),
            P(None, "tp"),
            P(None, "tp"),
            P(None, "tp"),
            P("tp"),
            P("tp", None),
            P("ep", None, "tp", None),
            P("ep", "tp", None),
            P("ep"),
            P(),
            P("ep", None),
            P("ep", None),
            P("ep", None, "tp"),
            P("ep", None, "tp"),
            P("ep", "tp", None),
            P(None, "ep"),
            P(None, "ep"),
            P("ep", None),
            P(),
        ),
        out_specs=P(("ep", "tp"), None),
        check_vma=False,
    )
```

time: 202 us -> 95.1 us (0.47)
  waiting for transfers between devices: 89.9 us -> 0 us
  Pallas kernels: 0 us -> 75.8 us
  starting transfers between devices: 46.7 us -> 0 us
  matrix products: 27.1 us -> 6.88 us
  between operations: 13.8 us -> 0.27 us
  local copies, waits for them, and re-layouts: 18.2 us -> 6.55 us
    all_to_all x7 -> x0, waiting for transfers between devices: 89.2 us -> none  [the longest x2 33.2 us: copy_for_each(): lax.all_to_all(jnp.broadcast_to(shard[None], (peers, *shard.shape)), axis...]
    pallas_call x0 -> x1, Pallas kernels: none -> 75.8 us  [after_attention(): pl.pallas_call(functools.partial(layer_kernel, top), out_shape=jax.ShapeD...]
    all_to_all x7 -> x0, starting transfers between devices: 46.7 us -> none  [the longest x1 14.3 us: moved(): lax.all_to_all(group, axis, split_axis=split_dim, concat_axis=concat_dim,...]
    dot_general x6 -> x0, matrix products: 20.9 us -> none  [the longest x1 8.65 us: on_device(): jnp.dot(own_act, lax.all_gather(dense_down, 'ep', axis=0, tiled=True), pr...]
    convert_element_type x5 -> x0, local copies, waits for them, and re-layouts: 6.79 us -> none  [the longest x2 5.26 us: on_device(): partial_units.astype(jnp.bfloat16)]
    concatenate x0 -> x2, other arithmetic: none -> 3.44 us  [the longest x1 2.76 us: after_attention(): whi = jnp.concatenate([none, dense_gate, none, dense_up], axis=1)]
    reshape x7 -> x1, local copies, waits for them, and re-layouts: 2.95 us -> 0.65 us  [after_attention(): tokens.reshape(ny, rows4, d_model)]
    broadcast_in_dim x2 -> x1, local copies, waits for them, and re-layouts: 2.33 us -> 0.07 us  [after_attention(): none = jnp.zeros((d_model, units), bf16)]
  transfers between devices with their start and end apart: 8 -> 0, of which waited for: 7 -> 0; matrix products, arithmetic and copies ran while one was open for 21% -> 0% of each run, Pallas kernels for 0% -> 0%
where the time goes in v1:
time: 95.1 us; the launch traced here: 94.9 us
  Pallas kernels  75.8 us (80%)
  matrix products  6.88 us (7%)
  local copies, waits for them, and re-layouts  6.55 us (7%)
  other arithmetic  5.42 us (6%)
    pallas_call x1, Pallas kernels, after_attention(): pl.pallas_call(functools.partial(layer_kernel, top), out_shape=jax.ShapeD...  75.8 us
    dot_general x1, matrix products, on_device(): jnp.einsum('skgd,slkd->skgl', queries, kv_cache[..., :head_dim], preferre...  3.62 us
    concatenate x1, other arithmetic, after_attention(): whi = jnp.concatenate([none, dense_gate, none, dense_up], axis=1)  2.76 us
    unnamed x41, local copies, waits for them, and re-layouts  2.17 us
    gather x4, local copies, waits for them, and re-layouts, on_device(): last_gate = jnp.take_along_axis(log_gates, last_index, axis=2)  2.03 us

profile of v1, /device:TPU:1, one launch (start us, length us, event | category | flops | bytes accessed | tf_op | source)
XLA Modules:
  0.0 94.9 jit_solution(12410462396599308685)
XLA Ops:
  0.0 0.7 broadcast_add_fusion
  0.7 0.7 broadcast_compare_fusion
  1.4 0.1 copy.64
  1.5 0.1 reshape.275
  1.6 0.0 copy-start.2
  1.6 0.0 copy-start.3
  1.6 0.0 copy-start.7
  1.6 0.0 copy-start.15
  1.6 0.0 copy-start.16
  1.7 0.0 copy-start.11
  1.7 0.0 copy-start.1
  1.7 1.8 %gather_fusion = f32[32]{0:T(128)S(1)} fusion(f32[16,2,1024]{2,1,0:T(2,128)} %param.33, s32[32]{0:T(128)S(1)} %reshape.275), kind=kCustom, calls=%fused_computation | custom fusion | bytes 640 | tf_op jit(solution)/shard_map/jit(take_along_axis)/gather | solution.py:607
  3.5 0.1 gather.7
  3.5 0.1 fusion.39
  3.6 0.0 copy-done.2
  3.6 0.1 fusion.29
  3.8 0.2 convolution_convert_fusion.2
  4.0 0.1 reshape.267
  4.1 0.2 fusion.47
  4.3 0.1 copy.65
  4.4 0.1 iota_compare_fusion
  4.6 0.0 copy-start.12
  4.6 3.6 %fusion.57 = (f32[16,2]{1,0:T(8,128)S(1)}, f32[16,2,1024]{2,1,0:T(2,128)S(1)}) fusion(f32[16,2]{1,0:T(8,128)S(1)} %copy.65, f32[16,2,1024]{2,1,0:T(2,128)S(1)} %copy-done.1, f32[16,2]{1,0:T(8,128)S(1)} %fusion.39, bf16[16,2,64]{2,1,0:T(2,128)(2,1)S(1)} %reshape.267, bf16[16,1024,1,128]{3,1,2,0:T(8,128)(2,1)} %param.32, ...), kind=kOutput, calls=%fused_computation.72 | convolution fusion | flops 4390880 | bytes 4477312 | tf_op jit(solution)/shard_map/skgd,slkd->skgl/dot_general | solution.py:601
  8.2 0.2 fusion.22
  8.4 0.1 fusion.40
  8.6 0.2 fusion.21
  8.9 0.0 copy-start.6
  8.9 0.0 copy-start.4
  8.9 1.4 %fusion.18 = bf16[16,2,64]{2,1,0:T(2,128)(2,1)S(1)} fusion(bf16[16,1024,1,128]{3,1,2,0:T(8,128)(2,1)S(1)} %copy-done.12, f32[16,2,1024]{2,1,0:T(2,128)S(1)} %get-tuple-element.15, f32[16,2]{1,0:T(8,128)S(1)} %get-tuple-element.10, f32[16,64]{1,0:T(8,128)S(1)} %fusion.21, f32[16,2]{1,0:T(8,128)S(1)} %get-tuple-element.9), kind=kOutput, calls=%fused_computation.11 | convolution fusion | flops 4265984 | bytes 4333824 | tf_op jit(solution)/shard_map/skgl,slkd->skgd/dot_general | solution.py:622
  10.3 0.1 dot_general.33
  10.4 0.8 fusion.27.part
  11.2 0.1 copy.70
  11.3 0.1 copy.71
  11.4 0.2 convert_reduce_fusion
  11.6 0.1 copy.69
  11.7 0.1 copy.67
  11.8 0.7 fusion.46.meta
  12.5 0.3 copy.73
  12.8 0.3 copy.74
  13.1 0.0 copy-start.9
  13.1 0.0 copy-start.10
  13.1 0.1 broadcast_in_dim.59
  13.2 2.8 %pad_maximum_fusion.1 = (bf16[2048,256]{1,0:T(8,128)(2,1)}, bf16[2048,256]{1,0:T(8,128)(2,1)}) fusion(bf16[2048,64]{1,0:T(8,128)(2,1)S(1)} %copy.74, bf16[2048,64]{1,0:T(8,128)(2,1)S(1)} %broadcast_in_dim.59, bf16[2048,64]{1,0:T(8,128)(2,1)S(1)} %copy.73), kind=kLoop, calls=%fused_computation.21 | loop fusion | flops 8388608 | bytes 2883584 | tf_op jit(solution)/shard_map/concatenate | solution.py:485
  15.9 0.6 reshape.270.tok
  16.6 0.6 jit_solution_.6.gs
  17.2 0.6 jit_solution_.7.cb
  17.8 75.8 %layer.1 = bf16[4,2048]{1,0:T(4,128)(2,1)} custom-call(f32[4,4,2048]{2,1,0:T(4,128)} %fusion.27.part, bf16[4,4,2048]{2,1,0:T(4,128)(2,1)} %reshape.270.tok, f32[1,2048]{1,0:T(1,128)} %bitcast.48, bf16[16,128]{1,0:T(8,128)(2,1)} %fusion.46.meta, f32[1,2048]{1,0:T(1,128)} %bitcast.49, f32[8,1024]{1,0:T(8,128)} %jit_solution_.6.gs, f32[8,192]{1,0:T(8,128)} %jit_solution_.7.cb, ...), custom_call_target="tpu_custom_call" | custom-call | tf_op jit(solution)/shard_map/layer/pallas_call | solution.py:530
  93.6 1.3 %copy.84 = bf16[4,2048]{1,0:T(4,128)(2,1)} copy(bf16[4,2048]{1,0:T(4,128)(2,1)} %layer.1) | data formatting | bytes 32768
  (32 shorter events, 0.1 us)
Async XLA Ops:
  0.0 10.4 %copy-start = (bf16[128,2048]{1,0:T(8,128)(2,1)S(1)}, bf16[128,2048]{1,0:T(8,128)(2,1)}, u32[]{:S(2)}) copy-start(bf16[128,2048]{1,0:T(8,128)(2,1)} %param.31) | copy-start | bytes 1572868
  1.6 2.0 %copy-start.2 = (bf16[16,2048]{1,0:T(8,128)(2,1)S(1)}, bf16[16,2048]{1,0:T(8,128)(2,1)}, u32[]{:S(2)}) copy-start(bf16[16,2048]{1,0:T(8,128)(2,1)} %param.24) | copy-start | bytes 196612
  1.6 2.2 %copy-start.3 = (bf16[2048,128]{1,0:T(8,128)(2,1)S(1)}, bf16[2048,128]{1,0:T(8,128)(2,1)}, u32[]{:S(2)}) copy-start(bf16[2048,128]{1,0:T(8,128)(2,1)} %param.26) | copy-start | bytes 1572868
  1.6 2.2 %copy-start.7 = (f32[2048]{0:T(1024)S(1)}, f32[2048]{0:T(1024)}, u32[]{:S(2)}) copy-start(f32[2048]{0:T(1024)} %param.25) | copy-start | bytes 24580
  1.6 2.5 %copy-start.15 = (bf16[2048,2]{0,1:T(2,128)(2,1)S(1)}, bf16[2048,2]{0,1:T(2,128)(2,1)}, u32[]{:S(2)}) copy-start(bf16[2048,2]{0,1:T(2,128)(2,1)} %param.29) | copy-start | bytes 24580
  1.6 2.5 %copy-start.16 = (f32[2]{0:T(128)S(1)}, f32[2]{0:T(128)}, u32[]{:S(2)}) copy-start(f32[2]{0:T(128)} %param.30) | copy-start | bytes 28
  1.7 2.8 %copy-start.11 = (s32[16]{0:T(128)S(1)}, s32[16]{0:T(128)}, u32[]{:S(2)}) copy-start(s32[16]{0:T(128)} %param.34) | copy-start | bytes 196
  1.7 2.9 %copy-start.1 = (f32[16,2,1024]{2,1,0:T(2,128)S(1)}, f32[16,2,1024]{2,1,0:T(2,128)}, u32[]{:S(2)}) copy-start(f32[16,2,1024]{2,1,0:T(2,128)} %param.33) | copy-start | bytes 393220
  4.5 3.7 %copy-start.13 = (bf16[2048,64]{0,1:T(8,128)(2,1)S(1)}, bf16[2048,64]{0,1:T(8,128)(2,1)}, u32[]{:S(2)}) copy-start(bf16[2048,64]{0,1:T(8,128)(2,1)} %param.27) | copy-start | bytes 786436
  4.6 4.1 %copy-start.14 = (bf16[2048,64]{0,1:T(8,128)(2,1)S(1)}, bf16[2048,64]{0,1:T(8,128)(2,1)}, u32[]{:S(2)}) copy-start(bf16[2048,64]{0,1:T(8,128)(2,1)} %param.28) | copy-start | bytes 786436
  4.6 4.3 %copy-start.12 = (bf16[16,1024,1,128]{3,1,2,0:T(8,128)(2,1)S(1)}, bf16[16,1024,1,128]{3,1,2,0:T(8,128)(2,1)}, u32[]{:S(2)}) copy-start(bf16[16,1024,1,128]{3,1,2,0:T(8,128)(2,1)} %param.32) | copy-start | bytes 12582916
  8.9 2.4 %copy-start.8 = (f32[16,4]{0,1:T(4,128)S(1)}, f32[16,4]{0,1:T(4,128)}, u32[]{:S(2)}) copy-start(f32[16,4]{0,1:T(4,128)} %param.37) | copy-start | bytes 772
  8.9 2.5 %copy-start.6 = (s32[16,4]{0,1:T(4,128)S(1)}, s32[16,4]{0,1:T(4,128)}, u32[]{:S(2)}) copy-start(s32[16,4]{0,1:T(4,128)} %param.36) | copy-start | bytes 772
  8.9 3.6 %copy-start.4 = (bf16[2048,64]{0,1:T(8,128)(2,1)S(1)}, bf16[2048,64]{0,1:T(8,128)(2,1)}, u32[]{:S(2)}) copy-start(bf16[2048,64]{0,1:T(8,128)(2,1)} %param.41) | copy-start | bytes 786436
  8.9 3.9 %copy-start.5 = (bf16[2048,64]{0,1:T(8,128)(2,1)S(1)}, bf16[2048,64]{0,1:T(8,128)(2,1)}, u32[]{:S(2)}) copy-start(bf16[2048,64]{0,1:T(8,128)(2,1)} %param.42) | copy-start | bytes 786436
  13.1 3.5 %copy-start.9 = (f32[1024]{0:T(1024)S(1)}, f32[1024]{0:T(1024)}, u32[]{:S(2)}) copy-start(f32[1024]{0:T(1024)} %constant.45.clone) | copy-start | bytes 12292
  13.1 4.1 %copy-start.10 = (f32[192]{0:T(256)S(1)}, f32[192]{0:T(256)}, u32[]{:S(2)}) copy-start(f32[192]{0:T(256)} %constant.46.clone) | copy-start | bytes 2308

commit v2 on v0

v2 whole, which is shorter than its diff:
```python
import functools

import jax
import jax.numpy as jnp
from jax import lax
from jax.experimental import pallas as pl
from jax.experimental.pallas import tpu as pltpu
from jax.sharding import PartitionSpec as P

EPS = 1e-05
LIMIT = 7.0
ALPHA = 1.702
NZ, NX, NC = 8, 4, 2
CAP = 3
META = 128
MESH = pl.DeviceIdType.MESH


def clamped_unit(gate_pre, up_pre):
    capped = jnp.minimum(gate_pre, LIMIT)
    return capped * jax.nn.sigmoid(ALPHA * capped) * (jnp.clip(up_pre, -LIMIT, LIMIT) + 1.0)


def rms_scaled(values, gain_vec):
    return values * lax.rsqrt(jnp.mean(values * values, axis=-1, keepdims=True) + EPS) * gain_vec


def remote(src, dst, send_sem, recv_sem, **device):
    return pltpu.make_async_remote_copy(
        src_ref=src,
        dst_ref=dst,
        send_sem=send_sem,
        recv_sem=recv_sem,
        device_id=device,
        device_id_type=MESH,
    )


IN_NAMES = (
    "tok",
    "gain1",
    "gain2",
    "dmix",
    "wq",
    "wkt",
    "wvt",
    "fwt",
    "fbias",
    "lengths",
    "gates",
    "routing",
    "weight",
    "wout",
    "kv",
    "eg_hbm",
    "eu_hbm",
    "ed_hbm",
    "dgt",
    "dut",
    "dd_hbm",
)
VMEM_INPUTS = 13


class Refs:
    pass


def layer_kernel(names, top, *refs):
    r = Refs()
    for name, ref in zip(names, refs, strict=True):
        setattr(r, name, ref)
    seq, d_model = r.tok.shape
    ny = r.part.shape[0]
    rows4 = seq // ny
    nblk = NC * NZ * NX
    fq = d_model // ny
    nxc = NX * NC
    zrows = CAP * nxc
    slots = NZ * zrows
    per_z = NX * seq
    both_z = NC * per_z
    f32, bf16 = jnp.float32, jnp.bfloat16
    h_all = r.h_all
    ep = lax.axis_index("ep")
    t = lax.axis_index("tp")
    z = ep // nxc
    x = (ep // NC) % NX
    c = ep % NC

    def ep_at(zi, xi, ci):
        return (zi * NX + xi) * NC + ci

    def blk(ci, zi, xi):
        return (ci * NZ + zi) * NX + xi

    def yp(d):
        return lax.rem(t + d + ny, ny)

    def zp(d):
        return lax.rem(z + d + NZ, NZ)

    def xp(d):
        return lax.rem(x + d + NX, NX)

    def cp(d):
        return lax.rem(c + d, NC)

    def iota(shape, dim):
        return lax.broadcasted_iota(jnp.int32, shape, dim)

    def dot_nt(a, b):
        return lax.dot_general(a, b, (((1,), (1,)), ((), ())), preferred_element_type=f32)

    def dot(a, b):
        return jnp.dot(a, b, preferred_element_type=f32)

    y_order = sorted(range(1, ny), key=lambda d: -min(d, ny - d))

    barrier = pltpu.get_barrier_semaphore()
    plane = [(dt, dx, dc) for dt in range(ny) for dc in range(NC) for dx in range(NX)][1:]
    for dt, dx, dc in plane:
        pl.semaphore_signal(
            barrier,
            inc=1,
            device_id={"ep": ep_at(z, xp(dx), cp(dc)), "tp": yp(dt)},
            device_id_type=MESH,
        )
    for d in range(1, NZ):
        pl.semaphore_signal(
            barrier, inc=1, device_id={"ep": ep_at(zp(d), x, c)}, device_id_type=MESH
        )

    units = r.dgt.shape[0]
    kv_groups = 4
    per_group = seq // kv_groups
    kv_loads = [
        pltpu.make_async_copy(
            r.kv.at[pl.ds(i * per_group, per_group)],
            r.kvbuf.at[pl.ds(i * per_group, per_group)],
            r.kvsem.at[i],
        )
        for i in range(kv_groups)
    ]
    late = [
        (r.dd_hbm.at[:, pl.ds(pl.multiple_of(t * fq, fq), fq)], r.dd.at[NZ - 1]),
        (r.wout, r.wo),
        (r.dgt, r.wgu.at[pl.ds(0, units)]),
        (r.dut, r.wgu.at[pl.ds(units, units)]),
        (r.eg_hbm, r.eg),
        (r.eu_hbm, r.eu),
        (r.ed_hbm, r.ed),
    ]
    late = [pltpu.make_async_copy(src, dst, r.ldsem.at[i]) for i, (src, dst) in enumerate(late)]
    for load in kv_loads + late:
        load.start()

    sent = {}

    def go(key, src, dst, recv_sem, **device):
        remote(src, dst, getattr(r, key), recv_sem, **device).start()
        sent[key] = sent.get(key, 0) + 1

    def arrived(ref, recv_sem):
        remote(ref, ref, r.s_dd, recv_sem, ep=ep, tp=t).wait_recv()

    tok = r.tok[...].astype(f32)
    normed = rms_scaled(tok, r.gain1[...])
    normed = normed.astype(bf16)
    hd = r.wkt.shape[0]
    cache_len = r.kv.shape[1]
    scale = hd ** (-0.5)
    q = dot(normed, r.wq[...]).astype(bf16).astype(f32)
    r.wkv[:hd] = r.wkt[...]
    r.wkv[hd:] = r.wvt[...]
    kv_new = dot_nt(normed, r.wkv[...]).astype(bf16).astype(f32)
    low_lanes = iota((seq, 2 * hd), 1) < hd
    q_heads = [jnp.where(low_lanes, q, 0.0), jnp.where(low_lanes, pltpu.roll(q, hd, 1), 0.0)]
    wide = normed.astype(f32)
    pairs = 2 * seq
    of_pair = iota((pairs, seq), 0) == 2 * iota((pairs, seq), 1)
    of_pair1 = iota((pairs, seq), 0) == 2 * iota((pairs, seq), 1) + 1
    eye = jnp.where(iota((seq, seq), 0) == iota((seq, seq), 1), 1.0, 0.0)

    def to_pairs(first, second):
        rows = [jnp.sum(eye * v, axis=0, keepdims=True) for v in (first, second)]
        return jnp.sum(
            jnp.where(of_pair, rows[0], jnp.where(of_pair1, rows[1], 0.0)), axis=1, keepdims=True
        )

    of_heads = [jnp.where(m, 1.0, 0.0).astype(bf16) for m in (of_pair, of_pair1)]
    q_pairs = sum(dot(of_heads[h], q_heads[h].astype(bf16)) for h in range(2))
    kv_pairs = dot(of_heads[0] + of_heads[1], kv_new.astype(bf16))
    gate_new, own_exp = [], []
    for h in range(2):
        pre = jnp.sum(wide * r.fwt[h : h + 1, :].astype(f32), axis=-1, keepdims=True)
        pre = pre + r.fbias[0, h]
        gate_new.append(jnp.minimum(pre, 0.0) - jnp.log(1.0 + jnp.exp(-jnp.abs(pre))))
        own_exp.append(jnp.exp(jnp.sum(q_heads[h] * kv_new, axis=-1, keepdims=True) * scale))
    gate_new = to_pairs(*gate_new)
    own_exp = to_pairs(*own_exp)

    rt = r.routing[...].astype(f32)
    wt = r.weight[...]
    earlier = iota((seq, seq), 1) < iota((seq, seq), 0)
    lane = iota((seq, META), 1)
    meta = jnp.zeros((seq, META), f32)

    def column(row):
        return jnp.sum(eye * row, axis=-1, keepdims=True)

    for k in range(top):
        chosen = column(rt[k : k + 1])
        same = jnp.zeros((seq, seq), f32)
        for other in range(top):
            same = same + jnp.where((chosen == rt[other : other + 1]) & earlier, 1.0, 0.0)
        rank = jnp.sum(same, axis=-1, keepdims=True)
        value = column(wt[k : k + 1])
        high = value.astype(bf16).astype(f32)
        mid = (value - high).astype(bf16).astype(f32)
        parts = (4.0 * chosen + rank, high, mid, value - high - mid)
        for i, v in enumerate(parts):
            meta = jnp.where(lane == i * top + k, v, meta)

    position = iota((8, cache_len), 1)
    row_pair = iota((8, 1), 0) // 2
    row_pair_wide = iota((8, 2 * hd), 0) // 2

    for g in range(kv_groups):
        kv_loads[g].wait()
        if g == kv_groups // 2:
            pl.semaphore_wait(barrier, len(plane) + (NZ - 1))
            late[0].wait()
            for d in range(1, NZ):
                go("s_dd", r.dd.at[NZ - 1], r.dd.at[d - 1], r.ddr, ep=ep_at(zp(d), x, c))
        at = slice(8 * g, 8 * g + 8)
        queries = q_pairs[at]
        scores = jnp.zeros((8, cache_len), f32)
        length = jnp.zeros((8, 1), jnp.int32)
        for i in range(4):
            only = jnp.where(row_pair_wide == i, queries, 0.0).astype(bf16)
            scores = scores + dot_nt(only, r.kvbuf[4 * g + i])
            length = jnp.where(row_pair == i, r.lengths[4 * g + i], length)
        gates = jnp.concatenate([r.gates[4 * g + i] for i in range(4)], axis=0)
        last_gate = jnp.sum(
            jnp.where(position == length - 1, gates, 0.0), axis=-1, keepdims=True
        )
        bias = last_gate - gates + gate_new[at]
        cached = jnp.where(position < length, jnp.exp(scores * scale + bias), 0.0)
        whole = jnp.sum(cached, axis=-1, keepdims=True) + own_exp[at]
        probs = (cached / whole).astype(bf16)
        got = (own_exp[at] / whole).astype(bf16).astype(f32) * kv_pairs[at]
        for i in range(4):
            got = got + jnp.where(row_pair_wide == i, dot(probs, r.kvbuf[4 * g + i]), 0.0)
        r.att[at] = got
    attended = jnp.where(
        low_lanes,
        pltpu.roll(r.att[pl.ds(0, seq, stride=2)], hd, 1),
        r.att[pl.ds(1, seq, stride=2)],
    ).astype(bf16)
    late[1].wait()

    r.part[ny - 1] = dot(attended, r.wo[...]).astype(bf16)
    for d in y_order:
        go("s_part", r.part.at[ny - 1], r.part.at[d - 1], r.s1r, tp=yp(d))
    arrived(r.part.at[pl.ds(0, ny - 1)], r.s1r)
    total = jnp.zeros((seq, d_model), f32)
    for j in range(ny):
        total = total + r.part[yp(-j - 1)].astype(f32)
    res = r.tok[...].astype(f32) + total.astype(bf16).astype(f32)
    for j in range(ny):
        r.resid[j] = res[j * rows4 : (j + 1) * rows4]
    mine = h_all.at[blk(c, z, x)]
    hidden = rms_scaled(res, r.gain2[...]).astype(bf16)
    common = d_model // 2
    lanes_tp = fq // 2
    wide_at = common + META
    mine[:, :common] = hidden[:, :common]
    mine[:, common:wide_at] = meta.astype(bf16)
    for j in range(ny):
        r.hid[j] = hidden[:, common + j * lanes_tp : common + (j + 1) * lanes_tp]
    mine[:, wide_at:] = r.hid[t]

    for d in range(1, NX):
        go("s_x", mine, mine, r.xrs.at[d - 1], ep=ep_at(z, xp(d), c))

    half = (NX + 1) // 2
    last = NZ // 2

    def takes(direction, step, q):
        if step < last:
            return True
        return q < half if direction > 0 else q >= half

    def pass_on(direction, step, q):
        if step > last or not takes(direction, step, q):
            return
        block = h_all.at[blk(c, zp(-direction * (step - 1)), xp(-q))]
        rs = r.rrs if direction > 0 else r.lrs
        go("s_ring", block, block, rs.at[step - 1, q], ep=ep_at(zp(direction), x, c))

    def across(rel, q):
        block = h_all.at[blk(c, zp(rel), xp(-q))]
        go("s_core", block, block, r.dcr.at[rel % NZ], ep=ep_at(z, x, cp(1)))

    others = pl.ds(1, ny - 1)

    def row_at(ci, rel):
        return pl.ds(blk(ci, zp(rel), 0), NX)

    def give_tp(rel):
        here = h_all.at[row_at(c, rel), :, pl.ds(wide_at, lanes_tp)]
        for d in y_order:
            go("s_tp", here, r.h_tp.at[d, row_at(c, rel)], r.tpr.at[rel % NZ], tp=yp(d))

    def take_tp(rel):
        there = r.h_tp.at[others, row_at(c, rel)]
        arrived(there, r.tpr.at[rel % NZ])
        go("s_tpcore", there, there, r.dtr.at[rel % NZ], ep=ep_at(z, x, cp(1)))

    def from_other_core(rel):
        arrived(h_all.at[row_at(cp(1), rel)], r.dcr.at[rel % NZ])
        arrived(r.h_tp.at[others, row_at(cp(1), rel)], r.dtr.at[rel % NZ])
        for ci in range(NC):
            at = pl.ds(blk(ci, zp(rel), 0), NX)
            r.h_tp[0, at] = h_all[at, :, wide_at:]

    def z_step(step):
        for q in range(NX):
            for direction in (1, -1):
                if not takes(direction, step, q):
                    continue
                rs = r.rrs if direction > 0 else r.lrs
                arrived(h_all.at[blk(c, zp(-direction * step), xp(-q))], rs.at[step - 1, q])
                pass_on(direction, step + 1, q)
                across(-direction * step, q)

    def features_of(zi):
        rows = []
        for ci in range(NC):
            at = pl.ds(blk(ci, zi, 0), NX)
            parts = [h_all[at, :, :common]] + [r.h_tp[yp(-j), at] for j in range(ny)]
            rows.append(jnp.concatenate(parts, axis=-1).reshape(per_z, d_model))
        return jnp.concatenate(rows, axis=0)

    def codes_of(zi):
        parts = [h_all[pl.ds(blk(ci, zi, 0), NX), :, common:wide_at] for ci in range(NC)]
        return jnp.concatenate([v.reshape(per_z, META) for v in parts], axis=0)

    in_first = iota((per_z, 2 * units), 1) < units

    def dense_units(rel):
        zi = zp(rel)
        pre = dot_nt(features_of(zi), r.wgu[...])
        low, high = pre[:per_z], pre[per_z:]
        act = clamped_unit(
            jnp.where(in_first, low, pltpu.roll(high, units, 1)),
            jnp.where(in_first, pltpu.roll(low, units, 1), high),
        ).astype(bf16)
        d = rel % NZ
        if d == 0:
            r.arecv[NZ - 1] = act
            return
        r.asend[d - 1] = act
        go("s_act", r.asend.at[d - 1], r.arecv.at[d - 1], r.ars, ep=ep_at(zi, x, c))

    lead8 = jnp.where(iota((8, META), 0) == iota((8, META), 1), 1.0, 0.0).astype(bf16)
    code_base = (ep * 4).astype(f32)

    def pick_rows(rel):
        zi = zp(rel)
        codes = dot_nt(lead8, codes_of(zi))
        block = iota((1, both_z), 1) // seq
        where = ((block % NX) * NC + block // NX).astype(f32)
        target = jnp.full((1, both_z), -1.0, f32)
        for k in range(top):
            j = codes[k : k + 1] - code_base
            target = jnp.where((j >= 0.0) & (j <= CAP - 1.0), where + j * nxc, target)
        slot = iota((zrows, both_z), 0).astype(f32)
        return dot(jnp.where(slot == target, 1.0, 0.0).astype(bf16), features_of(zi))

    def experts_of(rels, send=True):
        start = min(i for i, rel in enumerate(z_order) if rel in rels) * zrows
        rows = len(rels) * zrows
        for i, rel in enumerate(rels):
            r.xs[start + i * zrows : start + (i + 1) * zrows] = pick_rows(rel)
        xs = r.xs[start : start + rows].astype(bf16)
        act = clamped_unit(dot(xs, r.eg[...]), dot(xs, r.eu[...])).astype(bf16)
        for d in y_order + [0]:
            peer = yp(d)
            made = dot(act, r.ed[:, pl.ds(pl.multiple_of(peer * fq, fq), fq)])
            for i, rel in enumerate(rels):
                piece = made[i * zrows : (i + 1) * zrows]
                if d == 0:
                    r.rown[rel % NZ] = piece
                    continue
                r.ysend[d - 1, rel % NZ] = piece.astype(bf16)
            if d and send:
                send_results(rels, d)

    def send_results(rels, d):
        for rel in rels:
            i = rel % NZ
            go("s_y", r.ysend.at[d - 1, i], r.yrecv.at[i, d - 1], r.yrs.at[i], tp=yp(d))

    def finish(rels):
        for rel in rels:
            d = rel % NZ
            arrived(r.yrecv.at[d], r.yrs.at[d])
            summed = r.rown[d]
            for i in range(ny - 1):
                summed = summed + r.yrecv[d, i].astype(f32)
            if d == 0:
                r.zr[NZ - 1] = summed.astype(bf16)
                continue
            r.zs[d - 1] = summed.astype(bf16)
            go("s_z", r.zs.at[d - 1], r.zr.at[d - 1], r.zrs, ep=ep_at(zp(d), x, c))

    z_order = [0]
    for step in range(1, last):
        z_order += [-step, step]
    z_order.append(last)

    for q in range(NX):
        if q:
            arrived(h_all.at[blk(c, z, xp(-q))], r.xrs.at[q - 1])
        pass_on(1, 1, q)
        pass_on(-1, 1, q)
        across(0, q)
    give_tp(0)
    for load in late[2:]:
        load.wait()
    z_step(1)
    give_tp(-1)
    if last > 1:
        give_tp(1)
    take_tp(0)

    parts = [[0, -1, 1], [-2, 2], [-3, 3, 4]] if NZ == 8 else [z_order]
    for step in range(2, last + 1):
        z_step(step)
        give_tp(-step)
        if step < last:
            give_tp(step)
        take_tp(1 - step)
        take_tp(step - 1)
        if NZ != 8:
            continue
        if step == 4:
            for d in y_order:
                send_results(parts[0], d)
        if step == 2:
            from_other_core(0)
            dense_units(0)
        elif step == 3:
            from_other_core(-1)
            from_other_core(1)
            dense_units(-1)
            dense_units(1)
            experts_of(parts[0], send=False)
        else:
            from_other_core(-2)
            from_other_core(2)
            experts_of(parts[1])
            dense_units(-2)
            dense_units(2)
    own_meta = codes_of(z).astype(f32)
    mix = jnp.sum(features_of(z).astype(f32) * r.dmix[...], axis=-1, keepdims=True)
    mix = jax.nn.sigmoid(mix)
    col = iota((1, slots), 1)
    col_block = col // nxc
    col_z = (col_block * 43) // 128
    targets = 4 * (col_z * nxc + x * NC + c) + (col_block - CAP * col_z)
    targets = targets.astype(f32)
    row_block = iota((both_z, 1), 0) // seq
    row_xc = (row_block % NX) * NC + row_block // NX
    spread = jnp.zeros((both_z, slots), f32)
    for k in range(top):
        weight = (
            own_meta[:, top + k : top + k + 1]
            + own_meta[:, 2 * top + k : 2 * top + k + 1]
            + own_meta[:, 3 * top + k : 3 * top + k + 1]
        )
        spread = spread + jnp.where(own_meta[:, k : k + 1] == targets, weight, 0.0)
    spread = jnp.where(row_xc == col % nxc, spread, 0.0)
    spread_high = spread.astype(bf16)
    spread_low = (spread - spread_high.astype(f32)).astype(bf16)

    take_tp(last)
    for rel in parts[-1]:
        from_other_core(rel)
    experts_of(parts[-1])
    for part in parts[:-1]:
        finish(part)
    for rel in reversed(z_order[5:] if NZ == 8 else z_order):
        dense_units(rel)

    finish(parts[-1])

    arrived(r.dd.at[pl.ds(0, NZ - 1)], r.ddr)
    arrived(r.arecv.at[pl.ds(0, NZ - 1)], r.ars)
    dense = jnp.zeros((both_z, fq), f32)
    for j in range(NZ):
        got = r.arecv[j].astype(f32)
        both = jnp.concatenate(
            [jnp.where(in_first, got, 0.0), jnp.where(in_first, 0.0, got)], axis=0
        ).astype(bf16)
        twice = jnp.concatenate([r.dd[j], r.dd[j]], axis=0)
        dense = dense + dot(both, twice)
    dense = mix * dense
    arrived(r.zr.at[pl.ds(0, NZ - 1)], r.zrs)
    for j in range(NZ):
        r.zf[j * zrows : (j + 1) * zrows] = r.zr[lax.rem(z - j - 1 + 2 * NZ, NZ)].astype(f32)
    results = r.zf[...].astype(bf16)
    mixed = dot(spread_high, results) + dot(spread_low, results) + dense
    for i in range(nxc * ny):
        r.cs[i] = mixed[i * rows4 : (i + 1) * rows4].astype(bf16)

    for i, (dt, dx, dc) in enumerate(plane):
        here = (cp(dc) * NX + xp(dx)) * ny + yp(dt)
        go(
            "s_out",
            r.cs.at[here],
            r.cr.at[i + 1],
            r.crs,
            ep=ep_at(z, xp(dx), cp(dc)),
            tp=yp(dt),
        )
    r.cr[0] = r.cs[(c * NX + x) * ny + t]
    res = r.resid[t]
    arrived(r.cr.at[pl.ds(1, len(plane))], r.crs)
    for j in range(ny):
        cols = slice(j * fq, (j + 1) * fq)
        moved = r.cr[pl.ds(yp(-j) * nxc, nxc)].astype(f32)
        r.out[:, cols] = (res[:, cols] + jnp.sum(moved, axis=0)).astype(bf16)
    sizes = dict(
        s_dd=r.dd,
        s_part=r.part,
        s_x=h_all,
        s_ring=h_all,
        s_core=h_all,
        s_tpcore=None,
        s_tp=None,
        s_act=r.asend,
        s_z=r.zs,
        s_out=r.cr,
    )
    for key, count in sent.items():
        if key == "s_y":
            whole = r.ysend
        elif key == "s_tp":
            whole = r.h_tp.at[others, pl.ds(0, NX * NZ)]
        elif key == "s_tpcore":
            whole = r.h_tp.at[others, pl.ds(0, NX * count)]
        else:
            whole = sizes[key].at[pl.ds(0, count)]
        remote(whole, whole, getattr(r, key), r.crs, ep=ep, tp=t).wait_send()


def on_device(
    tokens,
    norm1_gain,
    query_weight,
    key_weight,
    value_weight,
    forget_weight,
    forget_bias,
    out_weight,
    kv_cache,
    log_gates,
    lengths,
    norm2_gain,
    routing,
    route_weight,
    expert_gate,
    expert_up,
    expert_down,
    dense_gate,
    dense_up,
    dense_down,
    dense_mix,
):
    seq, d_model = tokens.shape
    top = routing.shape[1]
    ny = lax.axis_size("tp")
    rows4 = seq // ny
    ff = expert_gate.shape[2]
    units = dense_gate.shape[1]
    fq = d_model // ny
    nxc = NX * NC
    nblk = NC * NZ * NX
    zrows = CAP * nxc
    slots = NZ * zrows
    width = d_model // 2 + META + fq // 2
    last = NZ // 2
    f32, bf16 = jnp.float32, jnp.bfloat16
    hd2 = kv_cache.shape[3]
    vm = pltpu.VMEM

    def dma(*shape):
        return pltpu.SemaphoreType.DMA(shape) if shape else pltpu.SemaphoreType.DMA

    scratch = dict(
        h_all=vm((nblk, seq, width), bf16),
        h_tp=vm((ny, nblk, seq, fq // 2), bf16),
        hid=vm((ny, seq, fq // 2), bf16),
        kvbuf=vm((seq, kv_cache.shape[1], hd2), bf16),
        wkv=vm((hd2, d_model), bf16),
        wo=vm((hd2, d_model), bf16),
        att=vm((2 * seq, hd2), f32),
        part=vm((ny, seq, d_model), bf16),
        resid=vm((ny, rows4, d_model), f32),
        eg=vm((d_model, ff), bf16),
        eu=vm((d_model, ff), bf16),
        ed=vm((ff, d_model), bf16),
        wgu=vm((2 * units, d_model), bf16),
        dd=vm((NZ, units, fq), bf16),
        xs=vm((slots, d_model), f32),
        ysend=vm((ny - 1, NZ, zrows, fq), bf16),
        yrecv=vm((NZ, ny - 1, zrows, fq), bf16),
        rown=vm((NZ, zrows, fq), f32),
        zs=vm((NZ - 1, zrows, fq), bf16),
        zr=vm((NZ, zrows, fq), bf16),
        zf=vm((slots, fq), f32),
        asend=vm((NZ - 1, NX * seq, 2 * units), bf16),
        arecv=vm((NZ, NX * seq, 2 * units), bf16),
        cs=vm((nxc * ny, rows4, fq), bf16),
        cr=vm((nxc * ny, rows4, fq), bf16),
        kvsem=dma(4),
        ldsem=dma(7),
        s1r=dma(),
        xrs=dma(max(NX - 1, 1)),
        rrs=dma(last, NX),
        lrs=dma(last, NX),
        dcr=dma(NZ),
        tpr=dma(NZ),
        dtr=dma(NZ),
        ddr=dma(),
        yrs=dma(NZ),
        zrs=dma(),
        ars=dma(),
        crs=dma(),
        s_dd=dma(),
        s_part=dma(),
        s_x=dma(),
        s_ring=dma(),
        s_core=dma(),
        s_tp=dma(),
        s_tpcore=dma(),
        s_act=dma(),
        s_y=dma(),
        s_z=dma(),
        s_out=dma(),
    )
    in_vmem = pl.BlockSpec(memory_space=pltpu.VMEM)
    in_smem = pl.BlockSpec(memory_space=pltpu.SMEM)
    in_hbm = pl.BlockSpec(memory_space=pl.ANY)
    places = [in_vmem] * VMEM_INPUTS + [in_hbm] * (len(IN_NAMES) - VMEM_INPUTS)
    places[IN_NAMES.index("lengths")] = in_smem
    places[IN_NAMES.index("fbias")] = in_smem
    names = tuple(IN_NAMES) + ("out",) + tuple(scratch)
    return pl.pallas_call(
        functools.partial(layer_kernel, names, top),
        out_shape=jax.ShapeDtypeStruct((rows4, d_model), bf16),
        in_specs=places,
        out_specs=in_vmem,
        scratch_shapes=list(scratch.values()),
        compiler_params=pltpu.CompilerParams(
            collective_id=0, has_side_effects=True, vmem_limit_bytes=60 * 1024 * 1024
        ),
        name="layer",
    )(
        tokens,
        norm1_gain.reshape(1, d_model),
        norm2_gain.reshape(1, d_model),
        dense_mix.reshape(1, d_model),
        query_weight,
        key_weight.T,
        value_weight.T,
        forget_weight.T,
        forget_bias.reshape(1, -1),
        lengths,
        log_gates,
        routing.T,
        route_weight.T,
        out_weight,
        kv_cache.reshape(seq, kv_cache.shape[1], hd2),
        expert_gate[0],
        expert_up[0],
        expert_down[0],
        dense_gate.T,
        dense_up.T,
        dense_down,
    )


def solution(mesh):
    return jax.shard_map(
        on_device,
        mesh=mesh,
        in_specs=(
            P("ep", None),
            P(),
            P(None, "tp"),
            P(None, "tp"),
            P(None, "tp"),
            P(None, "tp"),
            P("tp"),
            P("tp", None),
            P("ep", None, "tp", None),
            P("ep", "tp", None),
            P("ep"),
            P(),
            P("ep", None),
            P("ep", None),
            P("ep", None, "tp"),
            P("ep", None, "tp"),
            P("ep", "tp", None),
            P(None, "ep"),
            P(None, "ep"),
            P("ep", None),
            P(),
        ),
        out_specs=P(("ep", "tp"), None),
        check_vma=False,
    )
```

time: 202 us -> 68.6 us (0.34)
  waiting for transfers between devices: 89.9 us -> 0 us
  Pallas kernels: 0 us -> 67.1 us
  starting transfers between devices: 46.7 us -> 0 us
  matrix products: 27.1 us -> 0 us
  local copies, waits for them, and re-layouts: 18.2 us -> 1.33 us
  between operations: 13.8 us -> 0.01 us
  other arithmetic: 5.16 us -> 0 us
    all_to_all x7 -> x0, waiting for transfers between devices: 89.2 us -> none  [the longest x2 33.2 us: copy_for_each(): lax.all_to_all(jnp.broadcast_to(shard[None], (peers, *shard.shape)), axis...]
    pallas_call x0 -> x1, Pallas kernels: none -> 67.1 us  [on_device(): pl.pallas_call(functools.partial(layer_kernel, names, top), out_shape=jax...]
    all_to_all x7 -> x0, starting transfers between devices: 46.7 us -> none  [the longest x1 14.3 us: moved(): lax.all_to_all(group, axis, split_axis=split_dim, concat_axis=concat_dim,...]
    dot_general x14 -> x0, matrix products: 27.1 us -> none  [the longest x1 8.65 us: on_device(): jnp.dot(own_act, lax.all_gather(dense_down, 'ep', axis=0, tiled=True), pr...]
    convert_element_type x5 -> x0, local copies, waits for them, and re-layouts: 6.79 us -> none  [the longest x2 5.26 us: on_device(): partial_units.astype(jnp.bfloat16)]
    gather x6 -> x0, local copies, waits for them, and re-layouts: 3.03 us -> none  [the longest x1 1.15 us: on_device(): hidden_in[source.reshape(-1)].reshape(experts, capacity, model_width)]
    reshape x7 -> x0, local copies, waits for them, and re-layouts: 2.95 us -> none  [the longest x1 1.28 us: on_device(): hidden_in[source.reshape(-1)].reshape(experts, capacity, model_width)]
    reduce_sum x7 -> x0, other arithmetic: 2.73 us -> none  [the longest x1 1.28 us: sent_and_summed(): return arrived.astype(jnp.float32).sum(axis=0)]
  transfers between devices with their start and end apart: 8 -> 0, of which waited for: 7 -> 0; matrix products, arithmetic and copies ran while one was open for 21% -> 0% of each run, Pallas kernels for 0% -> 0%
where the time goes in v2:
time: 68.6 us; the launch traced here: 68.4 us
  Pallas kernels  67.1 us (98%)
  local copies, waits for them, and re-layouts  1.33 us (2%)
    pallas_call x1, Pallas kernels, on_device(): pl.pallas_call(functools.partial(layer_kernel, names, top), out_shape=jax...  67.1 us

profile of v2, /device:TPU:1, one launch (start us, length us, event | category | flops | bytes accessed | tf_op | source)
XLA Modules:
  0.0 68.4 jit_solution(4648129675357397945)
XLA Ops:
  0.0 67.1 %layer.1 = bf16[4,2048]{1,0:T(4,128)(2,1)} custom-call(bf16[16,2048]{1,0:T(8,128)(2,1)} %refs_0_.1, f32[1,2048]{1,0:T(1,128)} %bitcast.23, f32[1,2048]{1,0:T(1,128)} %bitcast.24, f32[1,2048]{1,0:T(1,128)} %bitcast.25, bf16[2048,128]{1,0:T(8,128)(2,1)} %refs_4_.1, bf16[64,2048]{1,0:T(8,128)(2,1)} %bitcast.19, bf16[64,2048]{1,0:T(8,128)(2,1)} %bitcast.20, ...), custom_call_target="tpu_custom_call" | custom-call | tf_op jit(solution)/shard_map/layer/pallas_call | solution.py:662
  67.1 1.3 %copy.23 = bf16[4,2048]{1,0:T(4,128)(2,1)} copy(bf16[4,2048]{1,0:T(4,128)(2,1)} %layer.1) | data formatting | bytes 32768

commit v3 on v2

--- a/solution.py
+++ b/solution.py
@@ -41,9 +41,6 @@
     "gain1",
     "gain2",
     "dmix",
-    "wq",
-    "wkt",
-    "wvt",
     "fwt",
     "fbias",
     "lengths",
@@ -52,6 +49,9 @@
     "weight",
     "wout",
     "kv",
+    "wq_hbm",
+    "wkt",
+    "wvt",
     "eg_hbm",
     "eu_hbm",
     "ed_hbm",
@@ -59,7 +59,7 @@
     "dut",
     "dd_hbm",
 )
-VMEM_INPUTS = 13
+VMEM_INPUTS = 10
 
 
 class Refs:
@@ -117,6 +117,14 @@
 
     y_order = sorted(range(1, ny), key=lambda d: -min(d, ny - d))
 
+    hd = r.wkt.shape[0]
+    early = [
+        pltpu.make_async_copy(r.wq_hbm, r.wq, r.qsem.at[0]),
+        pltpu.make_async_copy(r.wkt, r.wkv.at[pl.ds(0, hd)], r.qsem.at[1]),
+        pltpu.make_async_copy(r.wvt, r.wkv.at[pl.ds(hd, hd)], r.qsem.at[2]),
+    ]
+    for load in early:
+        load.start()
     barrier = pltpu.get_barrier_semaphore()
     plane = [(dt, dx, dc) for dt in range(ny) for dc in range(NC) for dx in range(NX)][1:]
     for dt, dx, dc in plane:
@@ -167,12 +175,11 @@
     tok = r.tok[...].astype(f32)
     normed = rms_scaled(tok, r.gain1[...])
     normed = normed.astype(bf16)
-    hd = r.wkt.shape[0]
+    for load in early:
+        load.wait()
     cache_len = r.kv.shape[1]
     scale = hd ** (-0.5)
     q = dot(normed, r.wq[...]).astype(bf16).astype(f32)
-    r.wkv[:hd] = r.wkt[...]
-    r.wkv[hd:] = r.wvt[...]
     kv_new = dot_nt(normed, r.wkv[...]).astype(bf16).astype(f32)
     low_lanes = iota((seq, 2 * hd), 1) < hd
     q_heads = [jnp.where(low_lanes, q, 0.0), jnp.where(low_lanes, pltpu.roll(q, hd, 1), 0.0)]
@@ -228,7 +235,7 @@
 
     for g in range(kv_groups):
         kv_loads[g].wait()
-        if g == kv_groups // 2:
+        if g == 0:
             pl.semaphore_wait(barrier, len(plane) + (NZ - 1))
             late[0].wait()
             for d in range(1, NZ):
@@ -626,6 +633,8 @@
         arecv=vm((NZ, NX * seq, 2 * units), bf16),
         cs=vm((nxc * ny, rows4, fq), bf16),
         cr=vm((nxc * ny, rows4, fq), bf16),
+        wq=vm((d_model, hd2), bf16),
+        qsem=dma(3),
         kvsem=dma(4),
         ldsem=dma(7),
         s1r=dma(),
@@ -674,9 +683,6 @@
         norm1_gain.reshape(1, d_model),
         norm2_gain.reshape(1, d_model),
         dense_mix.reshape(1, d_model),
-        query_weight,
-        key_weight.T,
-        value_weight.T,
         forget_weight.T,
         forget_bias.reshape(1, -1),
         lengths,
@@ -685,6 +691,9 @@
         route_weight.T,
         out_weight,
         kv_cache.reshape(seq, kv_cache.shape[1], hd2),
+        query_weight,
+        key_weight.T,
+        value_weight.T,
         expert_gate[0],
         expert_up[0],
         expert_down[0],

time: 68.6 us -> 67 us (0.977)
  Pallas kernels: 67.1 us -> 65.5 us
    pallas_call x1, Pallas kernels: 67.1 us -> 65.5 us  [on_device(): pl.pallas_call(functools.partial(layer_kernel, names, top), out_shape=jax...]
where the time goes in v3:
time: 67 us; the launch traced here: 66.9 us
  Pallas kernels  65.5 us (98%)
  local copies, waits for them, and re-layouts  1.33 us (2%)
    pallas_call x1, Pallas kernels, on_device(): pl.pallas_call(functools.partial(layer_kernel, names, top), out_shape=jax...  65.5 us

profile of v3, /device:TPU:1, one launch (start us, length us, event | category | flops | bytes accessed | tf_op | source)
XLA Modules:
  0.0 66.9 jit_solution(4786400517363171851)
XLA Ops:
  0.0 65.5 %layer.1 = bf16[4,2048]{1,0:T(4,128)(2,1)} custom-call(bf16[16,2048]{1,0:T(8,128)(2,1)} %refs_0_.1, f32[1,2048]{1,0:T(1,128)} %bitcast.23, f32[1,2048]{1,0:T(1,128)} %bitcast.24, f32[1,2048]{1,0:T(1,128)} %bitcast.25, bf16[2,2048]{1,0:T(2,128)(2,1)} %bitcast.26, f32[1,2]{1,0:T(1,128)} %bitcast.29, s32[16]{0:T(128)} %refs_6_.1, f32[16,2,1024]{2,1,0:T(2,128)} %refs_7_.1, ...), custom_call_target="tpu_custom_call" | custom-call | tf_op jit(solution)/shard_map/layer/pallas_call | solution.py:671
  65.5 1.3 %copy.23 = bf16[4,2048]{1,0:T(4,128)(2,1)} copy(bf16[4,2048]{1,0:T(4,128)(2,1)} %layer.1) | data formatting | bytes 32768

commit v4 on v3

--- a/solution.py
+++ b/solution.py
@@ -443,7 +443,7 @@
         give_tp(1)
     take_tp(0)
 
-    parts = [[0, -1, 1], [-2, 2], [-3, 3, 4]] if NZ == 8 else [z_order]
+    parts = [[0, -1, 1], [-2, 2], [4, -3, 3]] if NZ == 8 else [z_order]
     for step in range(2, last + 1):
         z_step(step)
         give_tp(-step)
@@ -523,7 +523,10 @@
     for i in range(nxc * ny):
         r.cs[i] = mixed[i * rows4 : (i + 1) * rows4].astype(bf16)
 
-    for i, (dt, dx, dc) in enumerate(plane):
+    far_first = sorted(
+        enumerate(plane), key=lambda p: -(min(p[1][0], ny - p[1][0]) + min(p[1][1], NX - p[1][1]))
+    )
+    for i, (dt, dx, dc) in far_first:
         here = (cp(dc) * NX + xp(dx)) * ny + yp(dt)
         go(
             "s_out",

time: 67 us -> 67 us (level)
  no operation moved by 1% of the time
where the time goes in v4:
time: 67 us; the launch traced here: 66.8 us
  Pallas kernels  65.5 us (98%)
  local copies, waits for them, and re-layouts  1.33 us (2%)
    pallas_call x1, Pallas kernels, on_device(): pl.pallas_call(functools.partial(layer_kernel, names, top), out_shape=jax...  65.5 us

profile of v4, /device:TPU:1, one launch (start us, length us, event | category | flops | bytes accessed | tf_op | source)
XLA Modules:
  0.0 66.8 jit_solution(8929367859918560794)
XLA Ops:
  0.0 65.5 %layer.1 = bf16[4,2048]{1,0:T(4,128)(2,1)} custom-call(bf16[16,2048]{1,0:T(8,128)(2,1)} %refs_0_.1, f32[1,2048]{1,0:T(1,128)} %bitcast.23, f32[1,2048]{1,0:T(1,128)} %bitcast.24, f32[1,2048]{1,0:T(1,128)} %bitcast.25, bf16[2,2048]{1,0:T(2,128)(2,1)} %bitcast.26, f32[1,2]{1,0:T(1,128)} %bitcast.29, s32[16]{0:T(128)} %refs_6_.1, f32[16,2,1024]{2,1,0:T(2,128)} %refs_7_.1, ...), custom_call_target="tpu_custom_call" | custom-call | tf_op jit(solution)/shard_map/layer/pallas_call | solution.py:674
  65.5 1.3 %copy.23 = bf16[4,2048]{1,0:T(4,128)(2,1)} copy(bf16[4,2048]{1,0:T(4,128)(2,1)} %layer.1) | data formatting | bytes 32768
